TPU v7x, 256 devices: a whole 4x4x8 slice. The times are simulated.
256 devices in a mesh: sp: 64 (over z, x, core), tp: 4 (over y).
Axes of the slice: x: 4, y: 4, z: 8, core: 2. Of those that a mesh axis runs over, the one named last changes fastest.
Arguments:
- mixer_input: bfloat16 [32768, 2048], P('sp', 'tp'), may hold values from -6 to 6
- residual: bfloat16 [32768, 2048], P(('sp', 'tp')), may hold values from -6 to 6
- log_step: float32 [128], P('tp'), may hold values from -3.9 to -2.3
- rate_real: float32 [128, 64], P('tp'), may hold values from -1.5 to 0, as said below
- rate_imag: float32 [128, 64], P('tp'), may hold values from 2 to 30
- damping: float32 [32768, 128], P('sp', 'tp'), may hold values from -2 to 0, as said below
- in_map: float32 [2, 128, 64, 16], P(None, 'tp'), may hold values from -1 to 1
- out_map: float32 [2, 128, 16, 64], P(None, 'tp'), may hold values from -0.75 to 0.75
- skip: float32 [2048], P('tp'), may hold values from -3 to 3
- w_out: bfloat16 [2048, 2048], P('tp'), may hold values from -0.125 to 0.125
- norm_gain: float32 [2048], replicated, may hold values from 0.1 to 1.9
- w_act: bfloat16 [2048, 5632], P('sp', 'tp'), may hold values from -0.125 to 0.125
- w_lin: bfloat16 [2048, 5632], P('sp', 'tp'), may hold values from -0.125 to 0.125
- conv_taps: float32 [2, 3, 5632], P(None, None, 'tp'), may hold values from -3.5 to 3.5
- w_down: bfloat16 [5632, 2048], P('tp', 'sp'), may hold values from -0.078125 to 0.078125
Outputs:
- layer_out: bfloat16 [32768, 2048], P(('sp', 'tp'))
Inputs may be any that keep to these rules, and one draw needn't show every extreme that they name: `rate_real`: all entries negative. `damping`: all entries at most zero.
All inputs are finite; a program needn't handle non-finite values.
Results may differ from a plain program's by a relative error of at most 0.02.
Values may be sent and summed in bfloat16 or wider, within the bound.
A program may use at most 192 MiB of HBM per device.

v0:
```python
import functools

import jax
import jax.numpy as jnp
from jax import lax
from jax.experimental import pallas as pl
from jax.experimental.pallas import tpu as pltpu
from jax.sharding import Mesh
from jax.sharding import PartitionSpec as P

F32, BF16 = jnp.float32, jnp.bfloat16
NT = (((1,), (1,)), ((), ()))
TN = (((0,), (0,)), ((), ()))
Q, CH, PAIRS = 8, 64, 16
CONV = 3
SP = ("sp_0", "sp_1", "sp_2")
SP_TP = ("sp_0", "sp_1", "sp_2", "tp")

def iota(shape, dim):
    return lax.broadcasted_iota(jnp.int32, shape, dim)

def cmul(ar, ai, br, bi):
    return ar * br - ai * bi, ar * bi + ai * br

def split3(x):
    hi = x.astype(BF16)
    r = x - hi.astype(F32)
    mid = r.astype(BF16)
    lo = (r - mid.astype(F32)).astype(BF16)
    return hi, mid, lo

def block_swap(x):
    s = iota(x.shape, 1)
    g = iota(x.shape, 2) // 16
    for b in (4, 2, 1):
        sb, gb = (s // b) % 2, (g // b) % 2
        down = pltpu.roll(pltpu.roll(x, 16 * b, axis=2), 8 - b, axis=1)
        if b == 4:
            up = down
        else:
            up = pltpu.roll(pltpu.roll(x, 128 - 16 * b, axis=2), b, axis=1)
        x = jnp.where(sb == gb, x, jnp.where(sb == 0, down, up))
    return x

def paired(even, odd):
    return jnp.concatenate([even, odd], axis=1)


def mixer_phase(r, comm, hooks=None):
    def rows(ref):
        return paired(ref[pl.ds(0, PAIRS, stride=2), :], ref[pl.ds(1, PAIRS, stride=2), :])

    rr, ri = rows(r.rr), rows(r.ri)
    step = jnp.exp(rows(r.ls))
    lr, th = rr * step, ri * step
    cos, sin = jnp.cos(th), jnp.sin(th)
    mag, inv = jnp.exp(lr), jnp.exp(-lr)
    ar, ai = mag * cos, mag * sin
    den = rr * rr + ri * ri
    r.fac[0] = ((ar - 1.0) * rr + ai * ri) / den
    r.fac[1] = (ai * rr - (ar - 1.0) * ri) / den
    one, zero = jnp.ones_like(ar), jnp.zeros_like(ar)
    pr, pi, nr, ni = one, zero, one, zero
    for s in range(Q):
        at = pl.ds(s, PAIRS, stride=Q)
        r.pw[0, at, :], r.pw[1, at, :] = nr, ni
        r.pw[2, at, :], r.pw[3, at, :] = pr, pi
        pr, pi = cmul(pr, pi, ar, ai)
        nr, ni = cmul(nr, ni, inv * cos, -inv * sin)
    d = r.damp[...]
    lane = iota(d.shape, 1) % Q
    for sh in (1, 2, 4):
        d = d + jnp.where(lane >= sh, pltpu.roll(d, sh, axis=1), 0.0)
    ex = (iota((96, 512), 0) % 32 == iota((96, 512), 1) // 16).astype(F32).astype(BF16)
    for n, sign in enumerate((-1.0, 1.0)):
        parts = jnp.concatenate([p.astype(F32) for p in split3(jnp.exp(sign * d))], axis=0).astype(BF16)
        r.ex[n] = lax.dot_general(parts, ex, TN, preferred_element_type=F32)
    pick = (iota((CH, 512), 1) == Q * iota((CH, 512), 0) + Q - 1).astype(F32).astype(BF16)
    ends = sum(lax.dot_general(pick, p, NT, preferred_element_type=F32) for p in split3(d))
    ends = jnp.exp(ends)
    low = iota((CH, 128), 1) < 64
    for k in range(PAIRS):
        r.e7[pl.ds(k, CH, stride=PAIRS), :] = jnp.where(low, ends[:, 2 * k : 2 * k + 1], ends[:, 2 * k + 1 : 2 * k + 2])

    def spread(b, _):
        j, c = b // 8, b % 8
        at = pl.ds(pl.multiple_of(c * 64, 64), 64)
        lanes = pl.ds(pl.multiple_of(j * 128, 128), 128)
        v = r.u[at, lanes].astype(F32) * r.ex[0, at, lanes]
        r.z[pl.ds(pl.multiple_of(b * 64, 64), 64), :] = block_swap(v.reshape(8, 8, 128)).reshape(64, 128)
        return 0

    lax.fori_loop(0, 32, spread, 0)

    def group_rows(k):
        first = (k // 4) * 512 + (k % 4) * 2
        return pl.ds(first, CH, stride=8), pl.ds(first + 1, CH, stride=8)

    low = iota((128, 128), 1) < 64

    def stacked(re, im):
        top = jnp.concatenate([jnp.where(low, re, 0.0), jnp.where(low, im, 0.0)], axis=1)
        bottom = jnp.concatenate([jnp.where(low, 0.0, re), jnp.where(low, 0.0, im)], axis=1)
        return jnp.concatenate([top, bottom], axis=0).astype(BF16)

    def outer(which, k, br, bi):
        at = pl.ds(pl.multiple_of(k * Q, Q), Q)
        wr, wi = r.pw[which, at, :][:, None, :], r.pw[which + 1, at, :][:, None, :]
        br, bi = br[None], bi[None]
        re, im = cmul(wr, wi, br, bi)
        return re.reshape(128, 128), im.reshape(128, 128)

    def inputs_of(k):
        even, odd = group_rows(k)
        return jnp.concatenate([r.z[even, :], r.z[odd, :]], axis=1).astype(BF16)

    def states_in(k, _):
        br, bi = paired(r.inm[0, 2 * k], r.inm[0, 2 * k + 1]), paired(r.inm[1, 2 * k], r.inm[1, 2 * k + 1])
        br, bi = cmul(r.fac[0, pl.ds(k, 1), :], r.fac[1, pl.ds(k, 1), :], br, bi)
        p = stacked(*outer(0, k, br, bi))
        r.pb[k] = p
        s = jnp.dot(inputs_of(k), p, preferred_element_type=F32)
        at = pl.ds(k, CH, stride=PAIRS)
        r.sr[at, :] = s[:, :128]
        r.si[at, :] = s[:, 128:]
        return 0

    lax.fori_loop(0, PAIRS, states_in, 0, unroll=2)

    a2r, a2i = cmul(ar, ai, ar, ai)
    a4r, a4i = cmul(a2r, a2i, a2r, a2i)
    a8r, a8i = cmul(a4r, a4i, a4r, a4i)

    def advance(c, carry, keep):
        vr, vi, e_all = carry
        at = pl.ds(pl.multiple_of(c * PAIRS, PAIRS), PAIRS)
        e = r.e7[at, :]
        tr, ti = (vr + r.sr[at, :]) * e, (vi + r.si[at, :]) * e
        if keep:
            r.sr[at, :], r.si[at, :] = vr, vi
        vr, vi = cmul(a8r, a8i, tr, ti)
        return vr, vi, e_all * e

    vr, vi, e_all = lax.fori_loop(0, CH, functools.partial(advance, keep=False), (zero, zero, one), unroll=8)

    causal = (iota((256, 256), 0) // 16) % Q <= (iota((256, 256), 1) // 16) % Q

    def inside(k, _):
        cr, ci = paired(r.outm[0, 2 * k], r.outm[0, 2 * k + 1]), paired(r.outm[1, 2 * k], r.outm[1, 2 * k + 1])
        qr, qi = outer(2, k, cr, ci)
        q = stacked(qr, -qi)
        r.qb[k] = q
        m = lax.dot_general(r.pb[k], q, NT, preferred_element_type=F32)
        m = jnp.where(causal, m, 0.0).astype(BF16)
        out = jnp.dot(inputs_of(k), m, preferred_element_type=F32)
        even, odd = group_rows(k)
        r.y[even, :] = out[:, :128]
        r.y[odd, :] = out[:, 128:]
        return 0

    def inside_part(n):
        cuts = (0, 6, 12, 16)
        lax.fori_loop(cuts[n], cuts[n + 1], inside, 0, unroll=2)

    vr, vi = comm(ar, ai, vr, vi, e_all, inside_part)
    lax.fori_loop(0, CH, functools.partial(advance, keep=True), (vr, vi, one), unroll=8)

    def outputs(k, _):
        at = pl.ds(k, CH, stride=PAIRS)
        v = jnp.concatenate([r.sr[at, :], r.si[at, :]], axis=1).astype(BF16)
        out = lax.dot_general(v, r.qb[k], NT, preferred_element_type=F32)
        even, odd = group_rows(k)
        r.y[even, :] += out[:, :128]
        r.y[odd, :] += out[:, 128:]
        return 0

    lax.fori_loop(0, PAIRS, outputs, 0, unroll=2)

    def finish(b, _):
        j, c = b // 8, b % 8
        at = pl.ds(pl.multiple_of(c * 64, 64), 64)
        lanes = pl.ds(pl.multiple_of(j * 128, 128), 128)
        v = r.y[pl.ds(pl.multiple_of(b * 64, 64), 64), :]
        v = block_swap(v.reshape(8, 8, 128)).reshape(64, 128)
        mixed = v * r.ex[1, at, lanes] + r.skip[:, lanes] * r.u[at, lanes].astype(F32)
        r.act[at, lanes] = jax.nn.gelu(mixed).astype(BF16)
        return 0

    lax.fori_loop(0, 32, finish, 0)


def fold(acc, vr, vi, e, wr, wi, use):
    er, ei = cmul(wr * e, wi * e, acc[0], acc[1])
    return jnp.where(use, er + vr, acc[0]), jnp.where(use, ei + vi, acc[1]), jnp.where(use, acc[2] * e, acc[2])


def squared(w, times):
    for _ in range(times):
        w = cmul(*w, *w)
    return w


class Refs:
    def __init__(self, **named):
        self.__dict__.update(named)


MIXER_SCRATCH = dict(
    fac=pltpu.VMEM((2, PAIRS, 128), F32), pw=pltpu.VMEM((4, PAIRS * Q, 128), F32), ex=pltpu.VMEM((2, 512, 512), F32),
    e7=pltpu.VMEM((CH * PAIRS, 128), F32), z=pltpu.VMEM((2048, 128), F32), y=pltpu.VMEM((2048, 128), F32),
    pb=pltpu.VMEM((PAIRS, 256, 256), BF16), qb=pltpu.VMEM((PAIRS, 256, 256), BF16),
    sr=pltpu.VMEM((CH * PAIRS, 128), F32), si=pltpu.VMEM((CH * PAIRS, 128), F32),
)


EXCHANGE_SCRATCH = dict(
    mine=pltpu.VMEM((3, 3, PAIRS, 128), F32), got_c=pltpu.VMEM((1, 3, PAIRS, 128), F32), got_x=pltpu.VMEM((3, 3, PAIRS, 128), F32),
    got_z=pltpu.VMEM((7, 3, PAIRS, 128), F32), ssem=pltpu.SemaphoreType.DMA((11,)), rsem=pltpu.SemaphoreType.DMA((11,)),
)


def greet(groups):
    barrier = pltpu.get_barrier_semaphore()
    many = 0
    for axis, count in groups:
        me = lax.axis_index(axis)
        for d in range(1, count):
            pl.semaphore_signal(barrier, inc=1, device_id={axis: lax.rem(me + d, count)}, device_id_type=pl.DeviceIdType.MESH)
            many += 1
    pl.semaphore_wait(barrier, many)


def exchange(r, ar, ai, vr, vi, e, part):
    core, x, z = lax.axis_index("sp_2"), lax.axis_index("sp_1"), lax.axis_index("sp_0")

    def copies(level, axis, me, count, got, first):
        return [
            pltpu.make_async_remote_copy(
                src_ref=r.mine.at[level], dst_ref=got.at[d - 1], send_sem=r.ssem.at[first + d - 1], recv_sem=r.rsem.at[first + d - 1],
                device_id={axis: lax.rem(me + d, count)}, device_id_type=pl.DeviceIdType.MESH,
            )
            for d in range(1, count)
        ]

    def put(level, parts):
        for n, v in enumerate(parts):
            r.mine[level, n] = v

    def of(got, slot):
        return got[slot, 0], got[slot, 1], got[slot, 2]

    nothing = (jnp.zeros_like(vr), jnp.zeros_like(vr), jnp.ones_like(vr))
    w1 = squared((ar, ai), 9)
    w2 = squared(w1, 1)
    w8 = squared(w2, 2)
    own = (vr, vi, e)
    put(0, own)
    for c in copies(0, "sp_2", core, 2, r.got_c, 0):
        c.start()
    part(0)
    for c in copies(0, "sp_2", core, 2, r.got_c, 0):
        c.wait()
    other = of(r.got_c, 0)
    early = [jnp.where(core == 0, a, b) for a, b in zip(own, other)]
    late = [jnp.where(core == 0, b, a) for a, b in zip(own, other)]
    chip = fold(early, *late, *w1, True)
    put(1, chip)
    for c in copies(1, "sp_1", x, 4, r.got_x, 1):
        c.start()
    part(1)
    for c in copies(1, "sp_1", x, 4, r.got_x, 1):
        c.wait()
    total = nothing
    for d in (3, 2, 1):
        total = fold(total, *of(r.got_x, d - 1), *w2, d <= x)
    total = fold(total, *chip, *w2, True)
    for d in (3, 2, 1):
        total = fold(total, *of(r.got_x, d - 1), *w2, d > x)
    put(2, total)
    sends = copies(2, "sp_0", z, 8, r.got_z, 4)
    for d in range(1, 8):
        pl.when(z + d < 8)(sends[d - 1].start)
    part(2)
    for d in range(1, 8):
        pl.when(z + d < 8)(sends[d - 1].wait_send)
        pl.when(z >= d)(sends[d - 1].wait_recv)
    enter = nothing
    for d in range(7, 0, -1):
        enter = fold(enter, *of(r.got_z, d - 1), *w8, d <= z)
    for d in (3, 2, 1):
        enter = fold(enter, *of(r.got_x, d - 1), *w2, d <= x)
    enter = fold(enter, *other, *w1, core == 1)
    return enter[0], enter[1]

SCRATCH = {**MIXER_SCRATCH, **EXCHANGE_SCRATCH}


def mixer_kernel(u, damp, ls, rr, ri, inm, outm, skip, act, *scratch):
    r = Refs(u=u, damp=damp, ls=ls, rr=rr, ri=ri, inm=inm, outm=outm, skip=skip, act=act, **dict(zip(SCRATCH, scratch)))
    r.got_z[...] = jnp.zeros_like(r.got_z)
    greet((("sp_2", 2), ("sp_1", 4), ("sp_0", 8)))
    mixer_phase(r, functools.partial(exchange, r))


def mixer(mixer_input, log_step, rate_real, rate_imag, damping, in_map, out_map, skip):
    return pl.pallas_call(
        mixer_kernel,
        out_shape=jax.ShapeDtypeStruct(mixer_input.shape, BF16),
        in_specs=[pl.BlockSpec(memory_space=pltpu.VMEM)] * 8,
        out_specs=pl.BlockSpec(memory_space=pltpu.VMEM),
        scratch_shapes=list(SCRATCH.values()),
        compiler_params=pltpu.CompilerParams(collective_id=0, has_side_effects=True, vmem_limit_bytes=40 * 2**20),
        cost_estimate=pl.CostEstimate(flops=6 * 10**9, bytes_accessed=4 * 10**6, transcendentals=0),
        name="mixer",
    )(
        mixer_input, damping.T, jnp.broadcast_to(log_step[:, None], rate_real.shape), rate_real, rate_imag,
        in_map.transpose(0, 1, 3, 2), out_map, skip[None],
    )


def sent_together(arrays, axis, dim, along):
    widths = [a.shape[along] for a in arrays]
    both = jnp.concatenate(arrays, axis=along)
    result = lax.all_gather(both, axis, axis=dim, tiled=True)
    return tuple(jnp.split(result, [sum(widths[:k]) for k in range(1, len(widths))], axis=along))


def cut_along(array, dim, peers):
    before, after = (array.shape[:dim], array.shape[dim + 1 :])
    return jnp.moveaxis(array.reshape(*before, peers, -1, *after), dim, 0)


def sent_and_summed(array, axis, dim):
    parts = cut_along(array, dim, lax.axis_size(axis))
    arrived = lax.all_to_all(parts, axis, split_axis=0, concat_axis=0, tiled=True)
    return arrived.astype(jnp.float32).sum(axis=0)


def joined_along(parts, dim):
    shape = list(parts.shape[1:])
    shape[dim] *= parts.shape[0]
    return jnp.moveaxis(parts, 0, dim).reshape(shape)


def from_everyone(array, axis):
    copies = jnp.broadcast_to(array, (lax.axis_size(axis), *array.shape))
    return lax.all_to_all(copies, axis, split_axis=0, concat_axis=0, tiled=True)


def collect(array, axis, dim):
    return joined_along(from_everyone(array, axis), dim)


def from_behind(value, axis, steps):
    count = lax.axis_size(axis)
    initial, last = (max(0, -steps), min(count, count - steps))
    return lax.ppermute(value, axis, [(source, source + steps) for source in range(initial, last)])


def normalize(stream, norm_gain):
    stream_f = stream.astype(jnp.float32)
    scale = lax.rsqrt(jnp.mean(stream_f * stream_f, axis=-1, keepdims=True) + 1e-06)
    return (stream_f * scale * norm_gain).astype(jnp.bfloat16)


def causal_conv(act_pre, lin_pre, previous, taps):
    row_count, width = act_pre.shape
    act_pad = jnp.concatenate([previous[0], act_pre], axis=0).astype(jnp.float32)
    lin_pad = jnp.concatenate([previous[1], lin_pre], axis=0).astype(jnp.float32)
    act_conv = jnp.zeros((row_count, width), jnp.float32)
    lin_conv = jnp.zeros((row_count, width), jnp.float32)
    for offset in range(CONV):
        act_conv = act_conv + taps[0, offset][None, :] * act_pad[offset : offset + row_count]
        lin_conv = lin_conv + taps[1, offset][None, :] * lin_pad[offset : offset + row_count]
    return (jax.nn.silu(act_conv) * lin_conv).astype(jnp.bfloat16)


def per_device(
    mixer_input,
    residual,
    log_step,
    rate_real,
    rate_imag,
    damping,
    in_map,
    out_map,
    skip,
    w_out,
    norm_gain,
    w_act,
    w_lin,
    conv_taps,
    w_down,
):
    tokens_here = mixer_input.shape[0]
    act_full, lin_full = sent_together((w_act, w_lin), SP, 0, 1)
    down_full = lax.all_gather(w_down, SP, axis=1, tiled=True)
    activated = mixer(mixer_input, log_step, rate_real, rate_imag, damping, in_map, out_map, skip)
    block = activated
    projected = sent_and_summed(
        jnp.dot(block, w_out, preferred_element_type=jnp.float32).astype(jnp.bfloat16), "tp", 0
    )
    stream = (residual.astype(jnp.float32) + projected).astype(jnp.bfloat16)
    normed_all = collect(normalize(stream, norm_gain), "tp", 0)
    act_pre = jnp.dot(normed_all, act_full, preferred_element_type=jnp.float32).astype(jnp.bfloat16)
    lin_pre = jnp.dot(normed_all, lin_full, preferred_element_type=jnp.float32).astype(jnp.bfloat16)
    edge = tokens_here - (CONV - 1)
    previous = from_behind((act_pre[edge:], lin_pre[edge:]), SP, 1)
    hidden = causal_conv(act_pre, lin_pre, previous, conv_taps)
    block = hidden
    channel_sum = sent_and_summed(
        jnp.dot(block, down_full, preferred_element_type=jnp.float32).astype(jnp.bfloat16), "tp", 0
    )
    return (stream.astype(jnp.float32) + channel_sum).astype(jnp.bfloat16)


def solution(mesh):
    split = Mesh(mesh.devices.reshape(8, 4, 2, mesh.shape["tp"]), ("sp_0", "sp_1", "sp_2", "tp"))
    in_specs = (
        P(SP, "tp"),
        P(SP_TP, None),
        P("tp"),
        P("tp", None),
        P("tp", None),
        P(SP, "tp"),
        P(None, "tp", None, None),
        P(None, "tp", None, None),
        P("tp"),
        P("tp", None),
        P(),
        P(SP, "tp"),
        P(SP, "tp"),
        P(None, None, "tp"),
        P("tp", SP),
    )
    out_specs = P(SP_TP, None)
    return jax.shard_map(
        per_device, mesh=split, in_specs=in_specs, out_specs=out_specs, check_vma=False
    )
```

profile of v0, /device:TPU:1, one launch (start us, length us, event | category | flops | bytes accessed | tf_op | source)
XLA Modules:
  0.0 232.6 jit_solution(4647358906307474477)
XLA Ops:
  6.5 1.8 pad_maximum_fusion
  8.3 0.0 all-gather.5.cloned.1.call-start
  8.4 0.7 all-gather.5.cloned.1.call-update
  9.1 0.7 broadcast_in_dim.6.ls
  9.8 1.0 copy-done.1
  10.9 1.0 copy-done.2
  11.9 1.0 copy-done.3
  12.9 0.8 copy-done.4
  13.8 0.7 copy-done.5
  14.5 0.7 copy-done.6
  15.2 0.7 copy-done.7
  15.9 39.6 %mixer.1 = bf16[512,512]{1,0:T(8,128)(2,1)S(1)} custom-call(bf16[512,512]{1,0:T(8,128)(2,1)S(1)} %copy-done.1, f32[32,512]{1,0:T(8,128)S(1)} %bitcast.12, f32[32,64]{1,0:T(8,128)S(1)} %broadcast_in_dim.6.ls, f32[32,64]{1,0:T(8,128)S(1)} %copy-done.5, f32[32,64]{1,0:T(8,128)S(1)} %copy-done.6, f32[2,32,16,64]{3,2,1,0:T(8,128)S(1)} %bitcast.11, ...), custom_call_target="tpu_custom_call" | custom-call | flops 6000000000 | bytes 4000000 | tf_op jit(solution)/shard_map/mixer/pallas_call | solution.py:306
  55.5 1.3 convolution_convert_fusion
  56.8 27.1 %all_to_all.15 = bf16[4,128,2048]{2,1,0:T(8,128)(2,1)S(1)} all-to-all(bf16[4,128,2048]{2,1,0:T(8,128)(2,1)S(1)} %bitcast.15), channel_id=1, replica_groups=mesh['sp_0'=8,'sp_1'=4,'sp_2'=2,'tp'=4] {'tp'}, dimensions={0} | all-to-all | bytes 4194304 | tf_op jit(solution)/shard_map/all_to_all | solution.py:335
  83.9 0.4 convert_reduce_fusion.1
  84.3 0.2 fusion.17
  84.6 0.2 fusion.19
  84.8 1.6 broadcast_in_dim.16
  86.4 4.5 %all-to-all-start.1 = ((bf16[4,128,2048]{2,1,0:T(8,128)(2,1)}), bf16[4,128,2048]{2,1,0:T(8,128)(2,1)}, u32[]{:S(2)}, u32[]{:S(2)}) async-start(bf16[4,128,2048]{2,1,0:T(8,128)(2,1)} %broadcast_in_dim.16), calls=%async_computation.1 | async-start | bytes 4194304 | tf_op jit(solution)/shard_map/all_to_all | solution.py:347
  90.8 0.1 slice_reduce_fusion.5
  90.9 21.8 %all-to-all-done.1 = bf16[4,128,2048]{2,1,0:T(8,128)(2,1)} async-done(((bf16[4,128,2048]{2,1,0:T(8,128)(2,1)}), bf16[4,128,2048]{2,1,0:T(8,128)(2,1)}, u32[]{:S(2)}, u32[]{:S(2)}) %all-to-all-start.1) | async-done | bytes 2097184 | tf_op jit(solution)/shard_map/all_to_all | solution.py:347
  112.7 6.9 %fusion.4 = bf16[512,1408]{1,0:T(8,128)(2,1)S(1)} fusion(bf16[512,2048]{1,0:T(8,128)(2,1)} %bitcast.4, bf16[2048,2816]{1,0:T(8,128)(2,1)} %all-gather.3.cloned.1.call-done), kind=kOutput, calls=%fused_computation.6 | convolution fusion | flops 2953510912 | bytes 9306112 | tf_op jit(solution)/shard_map/dot_general | solution.py:405
  119.6 6.9 %collective-permute-start = (bf16[2,1408]{1,0:T(2,128)(2,1)S(1)}, bf16[2,1408]{1,0:T(2,128)(2,1)S(1)}, u32[]{:S(2)}, u32[]{:S(2)}) collective-permute-start(bf16[2,1408]{1,0:T(2,128)(2,1)S(1)} %slice.56), channel_id=1, source_target_pairs={{0,4},{4,8},{8,12},{12,16},{16,20},{20,24},{24,28},{28,32},{32,36}... | collective-permute-start | bytes 16904 | tf_op jit(solution)/shard_map/ppermute | solution.py:357
  126.5 5.0 %fusion.7 = bf16[512,1408]{1,0:T(8,128)(2,1)S(1)} fusion(bf16[512,2048]{1,0:T(8,128)(2,1)} %bitcast.4, bf16[2048,2816]{1,0:T(8,128)(2,1)S(1)} %copy-done.11), kind=kOutput, calls=%fused_computation.7 | convolution fusion | flops 2953510912 | bytes 9306112 | tf_op jit(solution)/shard_map/dot_general | solution.py:406
  131.6 2.1 collective-permute-start.1
  133.7 1.9 maximum_convert_fusion
  135.6 1.9 maximum_convert_fusion.1
  137.5 44.7 %all-gather.5.cloned.1.call-done = bf16[1408,2048]{0,1:T(8,128)(2,1)} async-done(((bf16[1408,32]{0,1:T(8,128)(2,1)}), bf16[1408,2048]{0,1:T(8,128)(2,1)}) %all-gather.5.cloned.1.call-update) | async-done | bytes 5767184 | tf_op jit(solution)/shard_map/all_gather | solution.py:397
  182.2 12.6 %convolution_convert_fusion.1 = bf16[512,2048]{1,0:T(8,128)(2,1)S(1)} fusion(bf16[1408,2048]{0,1:T(8,128)(2,1)} %all-gather.5.cloned.1.call-done, f32[514,1408]{1,0:T(8,128)} %maximum_convert_fusion.1, f32[514,1408]{1,0:T(8,128)} %maximum_convert_fusion, f32[1408]{0:T(1024)S(1)} %get-tuple-element.9, f32[1408]{0:T(1024)S(1)} %get-tuple-element.10, ...), kind=kOutput, calls=%fused_computation.9 | convolution fusion | flops 2965372928 | bytes 25199616 | tf_op jit(solution)/shard_map/dot_general | solution.py:412
  194.8 29.7 %all_to_all.16 = bf16[4,128,2048]{2,1,0:T(8,128)(2,1)S(1)} all-to-all(bf16[4,128,2048]{2,1,0:T(8,128)(2,1)S(1)} %bitcast.14), channel_id=1, replica_groups=mesh['sp_0'=8,'sp_1'=4,'sp_2'=2,'tp'=4] {'tp'}, dimensions={0} | all-to-all | bytes 4194304 | tf_op jit(solution)/shard_map/all_to_all | solution.py:335
  224.5 0.4 convert_reduce_fusion
  224.9 0.9 fusion.20
  (25 shorter events, 0.1 us)
Async XLA Ops:
  6.5 49.0 %copy-start = (bf16[512,2048]{1,0:T(8,128)(2,1)S(1)}, bf16[512,2048]{1,0:T(8,128)(2,1)}, u32[]{:S(2)}) copy-start(bf16[512,2048]{1,0:T(8,128)(2,1)} %param.24) | copy-start | bytes 6291460
  6.5 106.1 %all-gather.3.cloned.1.call-start = ((), (), s32[]{:S(2)}) async-start(), calls=%async_computation.3 | async-start | bytes 11714560 | tf_op jit(solution)/shard_map/all_gather | solution.py:324
  8.3 173.8 %all-gather.5.cloned.1.call-start = ((), (), s32[]{:S(2)}) async-start(), calls=%async_computation.4 | async-start | bytes 5857280 | tf_op jit(solution)/shard_map/all_gather | solution.py:397
  9.8 1.0 copy-start.1
  10.9 1.0 copy-start.2
  11.9 1.0 copy-start.3
  12.9 0.8 copy-start.4
  13.8 0.7 copy-start.5
  14.5 0.7 copy-start.6
  15.2 0.7 copy-start.7
  56.8 27.5 %copy-start.8 = (bf16[128,2048]{1,0:T(8,128)(2,1)S(1)}, bf16[128,2048]{1,0:T(8,128)(2,1)}, u32[]{:S(2)}) copy-start(bf16[128,2048]{1,0:T(8,128)(2,1)} %param.16) | copy-start | bytes 1572868
  83.9 0.7 copy-start.10
  84.8 6.1 %copy-start.9 = (f32[2,3,1408]{2,0,1:T(2,128)S(1)}, f32[2,3,1408]{2,0,1:T(2,128)}, u32[]{:S(2)}) copy-start(f32[2,3,1408]{2,0,1:T(2,128)} %param.28) | copy-start | bytes 101380
  86.4 26.3 %all-to-all-start.1 = ((bf16[4,128,2048]{2,1,0:T(8,128)(2,1)}), bf16[4,128,2048]{2,1,0:T(8,128)(2,1)}, u32[]{:S(2)}, u32[]{:S(2)}) async-start(bf16[4,128,2048]{2,1,0:T(8,128)(2,1)} %broadcast_in_dim.16), calls=%async_computation.1 | async-start | bytes 4194304 | tf_op jit(solution)/shard_map/all_to_all | solution.py:347
  112.7 13.9 %copy-start.11 = (bf16[2048,2816]{1,0:T(8,128)(2,1)S(1)}, bf16[2048,2816]{1,0:T(8,128)(2,1)}, u32[]{:S(2)}) copy-start(bf16[2048,2816]{1,0:T(8,128)(2,1)} %all-gather.3.cloned.1.call-done) | copy-start | bytes 34603012
  119.6 14.0 %collective-permute-start = (bf16[2,1408]{1,0:T(2,128)(2,1)S(1)}, bf16[2,1408]{1,0:T(2,128)(2,1)S(1)}, u32[]{:S(2)}, u32[]{:S(2)}) collective-permute-start(bf16[2,1408]{1,0:T(2,128)(2,1)S(1)} %slice.56), channel_id=1, source_target_pairs={{0,4},{4,8},{8,12},{12,16},{16,20},{20,24},{24,28},{28,32},{32,36}... | collective-permute-start | bytes 16904 | tf_op jit(solution)/shard_map/ppermute | solution.py:357
  131.6 4.1 %collective-permute-start.1 = (bf16[2,1408]{1,0:T(2,128)(2,1)S(1)}, bf16[2,1408]{1,0:T(2,128)(2,1)S(1)}, u32[]{:S(2)}, u32[]{:S(2)}) collective-permute-start(bf16[2,1408]{1,0:T(2,128)(2,1)S(1)} %slice.60), channel_id=1, source_target_pairs={{0,4},{4,8},{8,12},{12,16},{16,20},{20,24},{24,28},{28,32},{32,36}... | collective-permute-start | bytes 16904 | tf_op jit(solution)/shard_map/ppermute | solution.py:357
Sparse Core Ops, SparseCore 0:
  10.1 92.5 all-gather.2
  105.4 76.7 all-gather.4
where the time goes:
time: 233 us
  waiting for transfers between devices  67.1 us (29%)
  blocking collectives  56.8 us (24%)
  Pallas kernels  39.6 us (17%)
  matrix products  25.8 us (11%)
  between operations  13.6 us (6%)
  starting transfers between devices  13.5 us (6%)
  local copies, waits for them, and re-layouts  8.55 us (4%)
  other arithmetic  7.69 us (3%)
    all_to_all x2, blocking collectives, sent_and_summed(): lax.all_to_all(parts, axis, split_axis=0, concat_axis=0, tiled=True)  56.8 us
    all_gather x1, waiting for transfers between devices, per_device(): down_full = lax.all_gather(w_down, SP, axis=1, tiled=True)  44.7 us
    pallas_call x1, Pallas kernels, mixer(): pl.pallas_call(mixer_kernel, out_shape=jax.ShapeDtypeStruct(mixer_input.s...  39.6 us
    all_to_all x1, waiting for transfers between devices, from_everyone(): return lax.all_to_all(copies, axis, split_axis=0, concat_axis=0, tiled=True)  21.8 us
    dot_general x1, matrix products, per_device(): jnp.dot(block, down_full, preferred_element_type=jnp.float32)  12.6 us
    ppermute x2, starting transfers between devices, from_behind(): lax.ppermute(value, axis, [(source, source + steps) for source in range(i...  8.98 us
    dot_general x1, matrix products, per_device(): jnp.dot(normed_all, act_full, preferred_element_type=jnp.float32)  6.93 us
    unnamed x24, local copies, waits for them, and re-layouts  6.14 us
  transfers between devices with their start and end apart: 5, of which 2 were waited for; matrix products, arithmetic and copies ran while one was open for 9% of the time, Pallas kernels for 17%

commit v1 on v0

--- a/solution.py
+++ b/solution.py
@@ -12,9 +12,9 @@
 NT = (((1,), (1,)), ((), ()))
 TN = (((0,), (0,)), ((), ()))
 Q, CH, PAIRS = 8, 64, 16
-CONV = 3
 SP = ("sp_0", "sp_1", "sp_2")
 SP_TP = ("sp_0", "sp_1", "sp_2", "tp")
+MESH = pl.DeviceIdType.MESH
 
 def iota(shape, dim):
     return lax.broadcasted_iota(jnp.int32, shape, dim)
@@ -46,7 +46,7 @@
     return jnp.concatenate([even, odd], axis=1)
 
 
-def mixer_phase(r, comm, hooks=None):
+def mixer_phase(r, comm, at_point):
     def rows(ref):
         return paired(ref[pl.ds(0, PAIRS, stride=2), :], ref[pl.ds(1, PAIRS, stride=2), :])
 
@@ -82,6 +82,8 @@
     for k in range(PAIRS):
         r.e7[pl.ds(k, CH, stride=PAIRS), :] = jnp.where(low, ends[:, 2 * k : 2 * k + 1], ends[:, 2 * k + 1 : 2 * k + 2])
 
+    at_point(0)
+
     def spread(b, _):
         j, c = b // 8, b % 8
         at = pl.ds(pl.multiple_of(c * 64, 64), 64)
@@ -91,6 +93,7 @@
         return 0
 
     lax.fori_loop(0, 32, spread, 0)
+    at_point(1)
 
     def group_rows(k):
         first = (k // 4) * 512 + (k % 4) * 2
@@ -125,7 +128,10 @@
         r.si[at, :] = s[:, 128:]
         return 0
 
-    lax.fori_loop(0, PAIRS, states_in, 0, unroll=2)
+    lax.fori_loop(0, 8, states_in, 0, unroll=2)
+    at_point(2)
+    lax.fori_loop(8, PAIRS, states_in, 0, unroll=2)
+    at_point(3)
 
     a2r, a2i = cmul(ar, ai, ar, ai)
     a4r, a4i = cmul(a2r, a2i, a2r, a2i)
@@ -164,6 +170,7 @@
 
     vr, vi = comm(ar, ai, vr, vi, e_all, inside_part)
     lax.fori_loop(0, CH, functools.partial(advance, keep=True), (vr, vi, one), unroll=8)
+    at_point(4)
 
     def outputs(k, _):
         at = pl.ds(k, CH, stride=PAIRS)
@@ -175,18 +182,26 @@
         return 0
 
     lax.fori_loop(0, PAIRS, outputs, 0, unroll=2)
-
-    def finish(b, _):
-        j, c = b // 8, b % 8
+    at_point(5)
+
+    def finish(first, b, _):
+        j, c = b // 2, first + b % 2
         at = pl.ds(pl.multiple_of(c * 64, 64), 64)
         lanes = pl.ds(pl.multiple_of(j * 128, 128), 128)
-        v = r.y[pl.ds(pl.multiple_of(b * 64, 64), 64), :]
+        v = r.y[pl.ds(pl.multiple_of(j * 512 + c * 64, 64), 64), :]
         v = block_swap(v.reshape(8, 8, 128)).reshape(64, 128)
         mixed = v * r.ex[1, at, lanes] + r.skip[:, lanes] * r.u[at, lanes].astype(F32)
         r.act[at, lanes] = jax.nn.gelu(mixed).astype(BF16)
         return 0
 
-    lax.fori_loop(0, 32, finish, 0)
+    me = lax.axis_index("tp")
+    for d in (2, 1, 3, 0):
+        q = lax.rem(me + d, 4)
+        lax.fori_loop(0, 8, functools.partial(finish, 2 * q), 0)
+        if d:
+            to_rows(r, d).start()
+        else:
+            r.acts[me] = r.act[pl.ds(pl.multiple_of(me * 128, 128), 128), :]
 
 
 def fold(acc, vr, vi, e, wr, wi, use):
@@ -219,25 +234,22 @@
 )
 
 
-def greet(groups):
+def greet(groups, others):
     barrier = pltpu.get_barrier_semaphore()
-    many = 0
-    for axis, count in groups:
-        me = lax.axis_index(axis)
-        for d in range(1, count):
-            pl.semaphore_signal(barrier, inc=1, device_id={axis: lax.rem(me + d, count)}, device_id_type=pl.DeviceIdType.MESH)
-            many += 1
-    pl.semaphore_wait(barrier, many)
-
-
-def exchange(r, ar, ai, vr, vi, e, part):
+    peers = [{axis: lax.rem(lax.axis_index(axis) + d, count)} for axis, count in groups for d in range(1, count)] + others
+    for peer in peers:
+        pl.semaphore_signal(barrier, inc=1, device_id=peer, device_id_type=MESH)
+    pl.semaphore_wait(barrier, len(peers))
+
+
+def exchange(r, between, ar, ai, vr, vi, e, part):
     core, x, z = lax.axis_index("sp_2"), lax.axis_index("sp_1"), lax.axis_index("sp_0")
 
     def copies(level, axis, me, count, got, first):
         return [
             pltpu.make_async_remote_copy(
                 src_ref=r.mine.at[level], dst_ref=got.at[d - 1], send_sem=r.ssem.at[first + d - 1], recv_sem=r.rsem.at[first + d - 1],
-                device_id={axis: lax.rem(me + d, count)}, device_id_type=pl.DeviceIdType.MESH,
+                device_id={axis: lax.rem(me + d, count)}, device_id_type=MESH,
             )
             for d in range(1, count)
         ]
@@ -280,6 +292,7 @@
     sends = copies(2, "sp_0", z, 8, r.got_z, 4)
     for d in range(1, 8):
         pl.when(z + d < 8)(sends[d - 1].start)
+    between()
     part(2)
     for d in range(1, 8):
         pl.when(z + d < 8)(sends[d - 1].wait_send)
@@ -292,126 +305,329 @@
     enter = fold(enter, *other, *w1, core == 1)
     return enter[0], enter[1]
 
-SCRATCH = {**MIXER_SCRATCH, **EXCHANGE_SCRATCH}
-
-
-def mixer_kernel(u, damp, ls, rr, ri, inm, outm, skip, act, *scratch):
-    r = Refs(u=u, damp=damp, ls=ls, rr=rr, ri=ri, inm=inm, outm=outm, skip=skip, act=act, **dict(zip(SCRATCH, scratch)))
+def to_rows(r, d):
+    me = lax.axis_index("tp")
+    q = lax.rem(me + d, 4)
+    return pltpu.make_async_remote_copy(
+        src_ref=r.act.at[pl.ds(pl.multiple_of(q * 128, 128), 128), :], dst_ref=r.acts.at[me],
+        send_sem=r.rows_s.at[d - 1], recv_sem=r.rows_r.at[d - 1], device_id={"tp": q}, device_id_type=MESH,
+    )
+
+
+class Ring:
+    def __init__(self, axis, count, chunk, ssem, rsem, shared=None):
+        self.axis, self.count, self.chunk, self.ssem, self.rsem, self.shared = axis, count, chunk, ssem, rsem, shared
+        self.me, self.half = lax.axis_index(axis), count // 2
+
+    def place(self, steps):
+        return lax.rem(self.me + steps + self.count, self.count)
+
+    def copy(self, step, way, k, owner):
+        n = ((step - 1) * 2 + way) * 2 + k
+        sign = 1 - 2 * way
+        ref = self.chunk(self.place(owner), k)
+        return pltpu.make_async_remote_copy(
+            src_ref=ref, dst_ref=ref, send_sem=self.ssem.at[n], recv_sem=self.rsem.at[n],
+            device_id={self.axis: self.place(sign)}, device_id_type=MESH,
+        )
+
+    def sends(self, step, i):
+        return [self.copy(step, way, (i, 1 - i)[way], -(1 - 2 * way) * (step - 1)) for way in (0, 1)]
+
+    def begin(self):
+        for i in (0, 1):
+            for c in self.sends(1, i):
+                c.start()
+
+    def services(self):
+        return [(s, i) for s in range(1, self.half + 1) for i in (0, 1) if s < self.half or i == 0]
+
+    def partner_copy(self, step, way, k, core):
+        n = ((step - 1) * 2 + way) * 2 + k
+        ref = self.chunk(self.place(-(1 - 2 * way) * step), k, core)
+        me = lax.axis_index("sp_2")
+        return pltpu.make_async_remote_copy(
+            src_ref=ref, dst_ref=ref, send_sem=self.shared[0].at[n], recv_sem=self.shared[1].at[n],
+            device_id={"sp_2": 1 - me}, device_id_type=MESH,
+        )
+
+    def service(self, step, i):
+        for way in (0, 1):
+            k = (i, 1 - i)[way]
+            self.copy(step, way, k, -(1 - 2 * way) * step).wait_recv()
+            if step + 1 < self.half or (step + 1 == self.half and i == 0):
+                self.copy(step + 1, way, k, -(1 - 2 * way) * step).start()
+            if self.shared:
+                self.partner_copy(step, way, k, lax.axis_index("sp_2")).start()
+
+    def shared_wait(self):
+        me = lax.axis_index("sp_2")
+        for s, i in self.services():
+            for way in (0, 1):
+                self.partner_copy(s, way, (i, 1 - i)[way], 1 - me).wait_recv()
+
+    def drain(self):
+        me = lax.axis_index("sp_2")
+        for s, i in self.services():
+            for c in self.sends(s, i):
+                c.wait_send()
+            if self.shared:
+                for way in (0, 1):
+                    self.partner_copy(s, way, (i, 1 - i)[way], me).wait_send()
+
+
+def sems(n):
+    return pltpu.SemaphoreType.DMA((n,))
+
+
+LAYER_SCRATCH = dict(
+    act=pltpu.VMEM((512, 512), BF16), acts=pltpu.VMEM((4, 128, 512), BF16), rows_s=sems(3), rows_r=sems(3),
+    g=pltpu.VMEM((3, 8, 4, 2, 32, 1408), BF16), wo=pltpu.VMEM((4, 2, 2, 128, 2048), BF16), load=sems(4),
+    stream=pltpu.VMEM((128, 2048), BF16), normed=pltpu.VMEM((4, 2, 64, 2048), BF16),
+    pre=pltpu.VMEM((2, 528, 1408), BF16), hidden=pltpu.VMEM((128, 1408), BF16),
+    part=pltpu.VMEM((3, 2, 128, 1024), BF16), own=pltpu.VMEM((2, 128, 1024), F32),
+    far=pltpu.VMEM((2, 128, 1024), BF16), near=pltpu.VMEM((2, 2, 128, 1024), BF16),
+    ax_s=sems(8), ax_r=sems(8), bz_s=sems(16), bz_r=sems(16), az_s=sems(16), az_r=sems(16), bx_s=sems(8), bx_r=sems(8),
+    wy_s=sems(8), wy_r=sems(8), ny_s=sems(8), ny_r=sems(8), azp_s=sems(16), azp_r=sems(16), bxp_s=sems(8), bxp_r=sems(8),
+    wyp_s=sems(8), wyp_r=sems(8), half_s=sems(2), half_r=sems(2), halo_s=sems(1), halo_r=sems(1), sum_s=sems(6), sum_r=sems(6),
+)
+SCRATCH = {**MIXER_SCRATCH, **EXCHANGE_SCRATCH, **LAYER_SCRATCH}
+IN_VMEM = ("u", "damp", "ls", "rr", "ri", "inm", "outm", "skip", "residual", "gain", "taps")
+IN_HBM = ("w_act", "w_lin", "w_dn", "w_out")
+
+
+def layer_kernel(*refs):
+    names = (*IN_VMEM, *IN_HBM, "out", *SCRATCH)
+    r = Refs(**dict(zip(names, refs)))
+    core, x, z, y = (lax.axis_index(a) for a in ("sp_2", "sp_1", "sp_0", "tp"))
+    loads = [pltpu.make_async_copy(w, r.g.at[m, z, x, core], r.load.at[m]) for m, w in enumerate((r.w_act, r.w_lin, r.w_dn))]
+    loads += [pltpu.make_async_copy(r.w_out.at[pl.ds((2 * c + k) * 128, 128), :], r.wo.at[y, c, k], r.load.at[3]) for c in (0, 1) for k in (0, 1)]
+    for c in loads:
+        c.start()
     r.got_z[...] = jnp.zeros_like(r.got_z)
-    greet((("sp_2", 2), ("sp_1", 4), ("sp_0", 8)))
-    mixer_phase(r, functools.partial(exchange, r))
-
-
-def mixer(mixer_input, log_step, rate_real, rate_imag, damping, in_map, out_map, skip):
+    at = z * 8 + x * 2 + core
+
+    def position(n):
+        n = lax.rem(n, 64)
+        return {"sp_0": n // 8, "sp_1": lax.rem(n, 8) // 2, "sp_2": lax.rem(n, 2)}
+
+    following, previous = position(at + 1), position(at + 63)
+    greet((("sp_2", 2), ("sp_1", 4), ("sp_0", 8), ("tp", 4)), [following, previous])
+    for c in loads:
+        c.wait()
+
+    halves = (pl.ds(0, 768), pl.ds(768, 640))
+    upper, lower = pl.ds(0, 16), pl.ds(16, 16)
+    ax = Ring("sp_1", 4, lambda o, k: r.g.at[:, z, o, core, upper, halves[k]], r.ax_s, r.ax_r)
+    bz = Ring("sp_0", 8, lambda o, k: r.g.at[:, o, x, core, lower, halves[k]], r.bz_s, r.bz_r)
+    az = Ring("sp_0", 8, lambda o, k, c=core: r.g.at[:, o, pl.ds(2 * k, 2), c, upper, :], r.az_s, r.az_r, (r.azp_s, r.azp_r))
+    bx = Ring("sp_1", 4, lambda o, k, c=core: r.g.at[:, pl.ds(4 * k, 4), o, c, lower, :], r.bx_s, r.bx_r, (r.bxp_s, r.bxp_r))
+    wy = Ring("tp", 4, lambda o, k, c=core: r.wo.at[o, c, k], r.wy_s, r.wy_r, (r.wyp_s, r.wyp_r))
+    ny = Ring("tp", 4, lambda o, k: r.normed.at[o, k], r.ny_s, r.ny_r)
+
+    def half_copies(c):
+        return [
+            pltpu.make_async_remote_copy(
+                src_ref=ref, dst_ref=ref, send_sem=r.half_s.at[n], recv_sem=r.half_r.at[n], device_id={"sp_2": 1 - core}, device_id_type=MESH
+            )
+            for n, ref in enumerate((r.g.at[:, z, :, c, upper, :], r.g.at[:, :, x, c, lower, :]))
+        ]
+
+    wy.begin()
+    ax.begin()
+    bz.begin()
+
+    def at_point(n):
+        if n == 0:
+            ax.service(1, 0)
+            ax.service(1, 1)
+            bz.service(1, 0)
+            bz.service(1, 1)
+        elif n == 1:
+            bz.service(2, 0)
+            bz.service(2, 1)
+            ax.service(2, 0)
+        elif n == 2:
+            bz.service(3, 0)
+            bz.service(3, 1)
+        elif n == 3:
+            bz.service(4, 0)
+        elif n == 4:
+            wy.service(1, 0)
+        elif n == 5:
+            az.service(1, 0)
+            wy.service(1, 1)
+
+    def between():
+        az.begin()
+        bx.begin()
+        for c in half_copies(core):
+            c.start()
+
+    mixer_phase(r, functools.partial(exchange, r, between), at_point)
+    az.service(1, 1)
+    bx.service(1, 0)
+    wy.service(2, 0)
+    for d in (2, 1, 3):
+        to_rows(r, d).wait_recv()
+    wy.shared_wait()
+
+    def project(n, squares):
+        cols = pl.ds(pl.multiple_of(n * 256, 256), 256)
+        total = r.residual[:, cols].astype(F32)
+        total += sum(jnp.dot(r.acts[q], r.wo[q, :, :, :, cols].reshape(512, 256), preferred_element_type=F32) for q in range(4))
+        total = total.astype(BF16)
+        r.stream[:, cols] = total
+        total = total.astype(F32)
+        return squares + total * total
+
+    squares = lax.fori_loop(0, 8, project, jnp.zeros((128, 256), F32))
+    scale = lax.rsqrt(jnp.sum(squares, axis=1, keepdims=True) / 2048 + 1e-06)
+
+    def normalize(n, _):
+        cols = pl.ds(pl.multiple_of(n * 256, 256), 256)
+        v = (r.stream[:, cols].astype(F32) * scale * r.gain[:, cols]).astype(BF16)
+        r.normed[y, :, :, cols] = v.reshape(2, 64, 256)
+        return 0
+
+    lax.fori_loop(0, 8, normalize, 0)
+    ny.begin()
+    az.service(2, 0)
+    az.service(2, 1)
+    ny.service(1, 0)
+    bx.service(1, 1)
+    az.service(3, 0)
+    ny.service(1, 1)
+    az.service(3, 1)
+    bx.service(2, 0)
+    ny.service(2, 0)
+    az.service(4, 0)
+    for c in half_copies(1 - core):
+        c.wait_recv()
+    bx.shared_wait()
+    az.shared_wait()
+
+    def up(h, cols, m):
+        lhs = r.normed[pl.ds(2 * h, 2)].reshape(256, 2048)
+        w = r.g[m, :, :, :, :, cols].reshape(2048, cols.size)
+        out = jnp.dot(lhs, w, preferred_element_type=F32)
+        r.pre[m, pl.ds(16 + 256 * h, 256), cols] = out.astype(BF16)
+
+    def up_half(h):
+        def tile(b, _):
+            up(h, pl.ds(pl.multiple_of((b // 2) * 256, 256), 256), b % 2)
+            return 0
+
+        lax.fori_loop(0, 10, tile, 0)
+        up(h, pl.ds(1280, 128), 0)
+        up(h, pl.ds(1280, 128), 1)
+
+    halo = pltpu.make_async_remote_copy(
+        src_ref=r.pre.at[:, pl.ds(512, 16), :], dst_ref=r.pre.at[:, pl.ds(0, 16), :], send_sem=r.halo_s.at[0], recv_sem=r.halo_r.at[0],
+        device_id=following, device_id_type=MESH,
+    )
+    up_half(1)
+    halo.start()
+    up_half(0)
+    halo.wait_recv()
+    starts = at == 0
+
+    def convolved(b, m, cols):
+        v = r.pre[m, pl.ds(pl.multiple_of(b * 128, 128), 144), cols].astype(F32)
+        v = jnp.where(jnp.logical_and(jnp.logical_and(starts, b == 0), iota(v.shape, 0) < 16), 0.0, v)
+        return sum(r.taps[k, pl.ds(m, 1), cols] * v[14 + k : 142 + k] for k in range(3))
+
+    def hide(b):
+        def tile(n, _):
+            cols = pl.ds(pl.multiple_of(n * 128, 128), 128)
+            a, l = convolved(b, 0, cols), convolved(b, 1, cols)
+            r.hidden[:, cols] = (a / (1.0 + jnp.exp(-a)) * l).astype(BF16)
+            return 0
+
+        lax.fori_loop(0, 11, tile, 0)
+
+    def down(put):
+        def tile(n, _):
+            w = r.g[2, pl.ds(n, 1)].reshape(256, 1408)
+            put(n // 4, pl.ds(pl.multiple_of((n % 4) * 256, 256), 256), lax.dot_general(r.hidden[...], w, NT, preferred_element_type=F32))
+            return 0
+
+        lax.fori_loop(0, 8, tile, 0)
+
+    def down_to(slot):
+        def put(side, cols, v):
+            r.part[slot, side, :, cols] = v.astype(BF16)
+
+        down(put)
+
+    def send_sum(n, src, dst, way):
+        return pltpu.make_async_remote_copy(
+            src_ref=src, dst_ref=dst, send_sem=r.sum_s.at[n], recv_sem=r.sum_r.at[n],
+            device_id={"tp": lax.rem(y + (1, 3)[way], 4)}, device_id_type=MESH,
+        )
+
+    def sums():
+        return [
+            send_sum(0, r.part.at[0, 0], r.far.at[0], 0),
+            send_sum(1, r.part.at[0, 1], r.far.at[1], 1),
+            send_sum(2, r.part.at[1, 1], r.near.at[0, 1], 0),
+            send_sum(3, r.part.at[2, 0], r.near.at[1, 0], 1),
+            send_sum(4, r.part.at[1, 0], r.near.at[0, 0], 0),
+            send_sum(5, r.part.at[2, 1], r.near.at[1, 1], 1),
+        ]
+
+    copies = sums()
+    hide(lax.rem(y + 2, 4))
+    down_to(0)
+    copies[0].start()
+    copies[1].start()
+    hide(lax.rem(y + 1, 4))
+    down_to(1)
+    copies[2].start()
+    hide(lax.rem(y + 3, 4))
+    down_to(2)
+    copies[3].start()
+    copies[0].wait_recv()
+    r.part[1, 0] = (r.part[1, 0].astype(F32) + r.far[0].astype(F32)).astype(BF16)
+    copies[4].start()
+    copies[1].wait_recv()
+    r.part[2, 1] = (r.part[2, 1].astype(F32) + r.far[1].astype(F32)).astype(BF16)
+    copies[5].start()
+    hide(y)
+
+    def keep(side, cols, v):
+        r.own[side, :, cols] = v
+
+    down(keep)
+    for c in copies[2:]:
+        c.wait_recv()
+    for side in (0, 1):
+        cols = pl.ds(side * 1024, 1024)
+        total = r.own[side] + r.near[0, side].astype(F32) + r.near[1, side].astype(F32)
+        r.out[:, cols] = (r.stream[:, cols].astype(F32) + total).astype(BF16)
+    for ring in (ax, bz, az, bx, wy, ny):
+        ring.drain()
+    for c in (*half_copies(core), *copies, halo, *(to_rows(r, d) for d in (1, 2, 3))):
+        c.wait_send()
+
+
+def per_device(
+    mixer_input, residual, log_step, rate_real, rate_imag, damping, in_map, out_map, skip, w_out, norm_gain, w_act, w_lin, conv_taps, w_down
+):
+    in_vmem = (
+        mixer_input, damping.T, jnp.broadcast_to(log_step[:, None], rate_real.shape), rate_real, rate_imag,
+        in_map.transpose(0, 1, 3, 2), out_map, skip[None], residual, norm_gain[None], conv_taps.transpose(1, 0, 2),
+    )
+    in_hbm = (w_act, w_lin, w_down.T, w_out)
     return pl.pallas_call(
-        mixer_kernel,
-        out_shape=jax.ShapeDtypeStruct(mixer_input.shape, BF16),
-        in_specs=[pl.BlockSpec(memory_space=pltpu.VMEM)] * 8,
+        layer_kernel,
+        out_shape=jax.ShapeDtypeStruct(residual.shape, BF16),
+        in_specs=[pl.BlockSpec(memory_space=pltpu.VMEM)] * len(in_vmem) + [pl.BlockSpec(memory_space=pl.ANY)] * len(in_hbm),
         out_specs=pl.BlockSpec(memory_space=pltpu.VMEM),
         scratch_shapes=list(SCRATCH.values()),
-        compiler_params=pltpu.CompilerParams(collective_id=0, has_side_effects=True, vmem_limit_bytes=40 * 2**20),
-        cost_estimate=pl.CostEstimate(flops=6 * 10**9, bytes_accessed=4 * 10**6, transcendentals=0),
-        name="mixer",
-    )(
-        mixer_input, damping.T, jnp.broadcast_to(log_step[:, None], rate_real.shape), rate_real, rate_imag,
-        in_map.transpose(0, 1, 3, 2), out_map, skip[None],
-    )
-
-
-def sent_together(arrays, axis, dim, along):
-    widths = [a.shape[along] for a in arrays]
-    both = jnp.concatenate(arrays, axis=along)
-    result = lax.all_gather(both, axis, axis=dim, tiled=True)
-    return tuple(jnp.split(result, [sum(widths[:k]) for k in range(1, len(widths))], axis=along))
-
-
-def cut_along(array, dim, peers):
-    before, after = (array.shape[:dim], array.shape[dim + 1 :])
-    return jnp.moveaxis(array.reshape(*before, peers, -1, *after), dim, 0)
-
-
-def sent_and_summed(array, axis, dim):
-    parts = cut_along(array, dim, lax.axis_size(axis))
-    arrived = lax.all_to_all(parts, axis, split_axis=0, concat_axis=0, tiled=True)
-    return arrived.astype(jnp.float32).sum(axis=0)
-
-
-def joined_along(parts, dim):
-    shape = list(parts.shape[1:])
-    shape[dim] *= parts.shape[0]
-    return jnp.moveaxis(parts, 0, dim).reshape(shape)
-
-
-def from_everyone(array, axis):
-    copies = jnp.broadcast_to(array, (lax.axis_size(axis), *array.shape))
-    return lax.all_to_all(copies, axis, split_axis=0, concat_axis=0, tiled=True)
-
-
-def collect(array, axis, dim):
-    return joined_along(from_everyone(array, axis), dim)
-
-
-def from_behind(value, axis, steps):
-    count = lax.axis_size(axis)
-    initial, last = (max(0, -steps), min(count, count - steps))
-    return lax.ppermute(value, axis, [(source, source + steps) for source in range(initial, last)])
-
-
-def normalize(stream, norm_gain):
-    stream_f = stream.astype(jnp.float32)
-    scale = lax.rsqrt(jnp.mean(stream_f * stream_f, axis=-1, keepdims=True) + 1e-06)
-    return (stream_f * scale * norm_gain).astype(jnp.bfloat16)
-
-
-def causal_conv(act_pre, lin_pre, previous, taps):
-    row_count, width = act_pre.shape
-    act_pad = jnp.concatenate([previous[0], act_pre], axis=0).astype(jnp.float32)
-    lin_pad = jnp.concatenate([previous[1], lin_pre], axis=0).astype(jnp.float32)
-    act_conv = jnp.zeros((row_count, width), jnp.float32)
-    lin_conv = jnp.zeros((row_count, width), jnp.float32)
-    for offset in range(CONV):
-        act_conv = act_conv + taps[0, offset][None, :] * act_pad[offset : offset + row_count]
-        lin_conv = lin_conv + taps[1, offset][None, :] * lin_pad[offset : offset + row_count]
-    return (jax.nn.silu(act_conv) * lin_conv).astype(jnp.bfloat16)
-
-
-def per_device(
-    mixer_input,
-    residual,
-    log_step,
-    rate_real,
-    rate_imag,
-    damping,
-    in_map,
-    out_map,
-    skip,
-    w_out,
-    norm_gain,
-    w_act,
-    w_lin,
-    conv_taps,
-    w_down,
-):
-    tokens_here = mixer_input.shape[0]
-    act_full, lin_full = sent_together((w_act, w_lin), SP, 0, 1)
-    down_full = lax.all_gather(w_down, SP, axis=1, tiled=True)
-    activated = mixer(mixer_input, log_step, rate_real, rate_imag, damping, in_map, out_map, skip)
-    block = activated
-    projected = sent_and_summed(
-        jnp.dot(block, w_out, preferred_element_type=jnp.float32).astype(jnp.bfloat16), "tp", 0
-    )
-    stream = (residual.astype(jnp.float32) + projected).astype(jnp.bfloat16)
-    normed_all = collect(normalize(stream, norm_gain), "tp", 0)
-    act_pre = jnp.dot(normed_all, act_full, preferred_element_type=jnp.float32).astype(jnp.bfloat16)
-    lin_pre = jnp.dot(normed_all, lin_full, preferred_element_type=jnp.float32).astype(jnp.bfloat16)
-    edge = tokens_here - (CONV - 1)
-    previous = from_behind((act_pre[edge:], lin_pre[edge:]), SP, 1)
-    hidden = causal_conv(act_pre, lin_pre, previous, conv_taps)
-    block = hidden
-    channel_sum = sent_and_summed(
-        jnp.dot(block, down_full, preferred_element_type=jnp.float32).astype(jnp.bfloat16), "tp", 0
-    )
-    return (stream.astype(jnp.float32) + channel_sum).astype(jnp.bfloat16)
+        compiler_params=pltpu.CompilerParams(collective_id=0, has_side_effects=True, vmem_limit_bytes=60 * 2**20),
+        name="layer",
+    )(*in_vmem, *in_hbm)
 
 
 def solution(mesh):

time: 233 us -> 127 us (0.55)
  Pallas kernels: 39.6 us -> 124 us
  waiting for transfers between devices: 67.1 us -> 0 us
  blocking collectives: 56.8 us -> 0 us
  matrix products: 25.8 us -> 0 us
  between operations: 13.6 us -> 0.01 us
  starting transfers between devices: 13.5 us -> 0 us
  other arithmetic: 7.69 us -> 0 us
  local copies, waits for them, and re-layouts: 8.55 us -> 3.21 us
    pallas_call x1, Pallas kernels: 39.6 us -> 124 us  [per_device(): pl.pallas_call(layer_kernel, out_shape=jax.ShapeDtypeStruct(residual.shap...]
    all_to_all x2 -> x0, blocking collectives: 56.8 us -> none  [sent_and_summed(): lax.all_to_all(parts, axis, split_axis=0, concat_axis=0, tiled=True)]
    all_gather x2 -> x0, waiting for transfers between devices: 44.7 us -> none  [the longest x1 44.7 us: per_device(): down_full = lax.all_gather(w_down, SP, axis=1, tiled=True)]
    dot_general x4 -> x0, matrix products: 25.8 us -> none  [the longest x1 12.6 us: per_device(): jnp.dot(block, down_full, preferred_element_type=jnp.float32)]
    all_to_all x1 -> x0, waiting for transfers between devices: 21.8 us -> none  [from_everyone(): return lax.all_to_all(copies, axis, split_axis=0, concat_axis=0, tiled=True)]
    ppermute x2 -> x0, starting transfers between devices: 8.98 us -> none  [from_behind(): lax.ppermute(value, axis, [(source, source + steps) for source in range(i...]
    convert_element_type x4 -> x0, other arithmetic: 4.91 us -> none  [the longest x1 1.93 us: causal_conv(): jnp.concatenate([previous[0], act_pre], axis=0).astype(jnp.float32)]
    all_to_all x1 -> x0, starting transfers between devices: 4.46 us -> none  [from_everyone(): return lax.all_to_all(copies, axis, split_axis=0, concat_axis=0, tiled=True)]
  transfers between devices with their start and end apart: 5 -> 0, of which waited for: 2 -> 0; matrix products, arithmetic and copies ran while one was open for 9% -> 0% of each run, Pallas kernels for 17% -> 0%
where the time goes in v1:
time: 127 us
  Pallas kernels  124 us (98%)
  local copies, waits for them, and re-layouts  3.21 us (3%)
    pallas_call x1, Pallas kernels, per_device(): pl.pallas_call(layer_kernel, out_shape=jax.ShapeDtypeStruct(residual.shap...  124 us

profile of v1, /device:TPU:1, one launch (start us, length us, event | category | flops | bytes accessed | tf_op | source)
XLA Modules:
  0.0 127.0 jit_solution(2366455426109982080)
XLA Ops:
  0.0 1.3 %broadcast_in_dim.12.refs_2_ = f32[32,64]{1,0:T(8,128)} broadcast(f32[32]{0:T(128)} %param.17), dimensions={0} | broadcast | bytes 8320 | tf_op jit(solution)/shard_map/broadcast_in_dim | solution.py:618
  1.3 123.8 %layer.1 = bf16[128,2048]{1,0:T(8,128)(2,1)} custom-call(bf16[512,512]{1,0:T(8,128)(2,1)} %refs_0_.1, f32[32,512]{1,0:T(8,128)} %bitcast.8, f32[32,64]{1,0:T(8,128)} %broadcast_in_dim.12.refs_2_, f32[32,64]{1,0:T(8,128)} %refs_3_.1, f32[32,64]{1,0:T(8,128)} %refs_4_.1, f32[2,32,16,64]{3,2,1,0:T(8,128)} %bitcast.6, f32[2,32,16,64]{3,2,1,0:T(8,128)} %refs_6_.1, ...), custom_call_target="tpu_custom_call" | custom-call | tf_op jit(solution)/shard_map/layer/pallas_call | solution.py:622
  125.2 1.9 %copy.17 = bf16[128,2048]{1,0:T(8,128)(2,1)} copy(bf16[128,2048]{1,0:T(8,128)(2,1)} %layer.1) | data formatting | bytes 1048576

commit v2 on v0

v2 whole, which is shorter than its diff:
```python
import functools

import jax
import jax.numpy as jnp
from jax import lax
from jax.experimental import pallas as pl
from jax.experimental.pallas import tpu as pltpu
from jax.sharding import Mesh
from jax.sharding import PartitionSpec as P

F32, BF16 = jnp.float32, jnp.bfloat16
NT = (((1,), (1,)), ((), ()))
TN = (((0,), (0,)), ((), ()))
Q, CH, PAIRS = 8, 64, 16
SP = ("sp_0", "sp_1", "sp_2")
SP_TP = ("sp_0", "sp_1", "sp_2", "tp")
MESH = pl.DeviceIdType.MESH

def iota(shape, dim):
    return lax.broadcasted_iota(jnp.int32, shape, dim)

def cmul(ar, ai, br, bi):
    return ar * br - ai * bi, ar * bi + ai * br

def split3(x):
    hi = x.astype(BF16)
    r = x - hi.astype(F32)
    mid = r.astype(BF16)
    lo = (r - mid.astype(F32)).astype(BF16)
    return hi, mid, lo

def block_swap(parts):
    parts = list(parts)
    block = iota(parts[0].shape, 1) // 16
    for b in (4, 2, 1):
        here = (block // b) % 2 == 0
        for n in range(8):
            if n & b == 0:
                low, high = parts[n], parts[n + b]
                parts[n] = jnp.where(here, low, pltpu.roll(high, 16 * b, axis=1))
                parts[n + b] = jnp.where(here, pltpu.roll(low, 128 - 16 * b, axis=1), high)
    return parts


def paired(even, odd):
    return jnp.concatenate([even, odd], axis=1)


def mixer_phase(r, greeted, comm, at_point):
    def rows(ref):
        return paired(ref[pl.ds(0, PAIRS, stride=2), :], ref[pl.ds(1, PAIRS, stride=2), :])

    rr, ri = rows(r.rr), rows(r.ri)
    step = jnp.exp(rows(r.ls))
    lr, th = rr * step, ri * step
    cos, sin = jnp.cos(th), jnp.sin(th)
    mag, inv = jnp.exp(lr), jnp.exp(-lr)
    ar, ai = mag * cos, mag * sin
    den = rr * rr + ri * ri
    r.fac[0] = ((ar - 1.0) * rr + ai * ri) / den
    r.fac[1] = (ai * rr - (ar - 1.0) * ri) / den
    one, zero = jnp.ones_like(ar), jnp.zeros_like(ar)
    pr, pi, nr, ni = one, zero, one, zero
    for s in range(Q):
        at = pl.ds(s, PAIRS, stride=Q)
        r.pw[0, at, :], r.pw[1, at, :] = nr, ni
        r.pw[2, at, :], r.pw[3, at, :] = pr, pi
        pr, pi = cmul(pr, pi, ar, ai)
        nr, ni = cmul(nr, ni, inv * cos, -inv * sin)
    d = r.damp[...]
    lane = iota(d.shape, 1) % Q
    for sh in (1, 2, 4):
        d = d + jnp.where(lane >= sh, pltpu.roll(d, sh, axis=1), 0.0)
    ex = (iota((96, 512), 0) % 32 == iota((96, 512), 1) // 16).astype(F32).astype(BF16)
    def spread_out(v):
        parts = jnp.concatenate([p.astype(F32) for p in split3(v)], axis=0).astype(BF16)
        return lax.dot_general(parts, ex, TN, preferred_element_type=F32)

    pick = (iota((CH, 512), 1) == Q * iota((CH, 512), 0) + Q - 1).astype(F32).astype(BF16)
    ends = sum(lax.dot_general(pick, p, NT, preferred_element_type=F32) for p in split3(d))
    ends = jnp.exp(ends)
    low = iota((CH, 128), 1) < 64
    for k in range(PAIRS):
        r.e7[pl.ds(k, CH, stride=PAIRS), :] = jnp.where(low, ends[:, 2 * k : 2 * k + 1], ends[:, 2 * k + 1 : 2 * k + 2])

    greeted()
    shrink = spread_out(jnp.exp(-d)) * r.u[...].astype(F32)
    for j in range(4):
        r.v[j] = shrink[:, j * 128 : j * 128 + 128]

    def spread(b, _):
        j, c = b // 2, b % 2
        parts = block_swap([r.v[j, pl.ds(c * 256 + n, 32, stride=8), :] for n in range(8)])
        for n in range(8):
            r.z[j * 8 + n, pl.ds(pl.multiple_of(c * 32, 32), 32), :] = parts[n]
        return 0

    lax.fori_loop(0, 8, spread, 0)

    low = iota((128, 128), 1) < 64

    def stacked(re, im):
        top = jnp.concatenate([jnp.where(low, re, 0.0), jnp.where(low, im, 0.0)], axis=1)
        bottom = jnp.concatenate([jnp.where(low, 0.0, re), jnp.where(low, 0.0, im)], axis=1)
        return jnp.concatenate([top, bottom], axis=0).astype(BF16)

    def outer(which, k, br, bi):
        at = pl.ds(pl.multiple_of(k * Q, Q), Q)
        wr, wi = r.pw[which, at, :][:, None, :], r.pw[which + 1, at, :][:, None, :]
        br, bi = br[None], bi[None]
        re, im = cmul(wr, wi, br, bi)
        return re.reshape(128, 128), im.reshape(128, 128)

    def inputs_of(k):
        return jnp.concatenate([r.z[2 * k], r.z[2 * k + 1]], axis=1).astype(BF16)

    def states_in(k, _):
        br, bi = paired(r.inm[0, 2 * k], r.inm[0, 2 * k + 1]), paired(r.inm[1, 2 * k], r.inm[1, 2 * k + 1])
        br, bi = cmul(r.fac[0, pl.ds(k, 1), :], r.fac[1, pl.ds(k, 1), :], br, bi)
        p = stacked(*outer(0, k, br, bi))
        r.pb[k] = p
        s = jnp.dot(inputs_of(k), p, preferred_element_type=F32)
        at = pl.ds(k, CH, stride=PAIRS)
        r.sr[at, :] = s[:, :128]
        r.si[at, :] = s[:, 128:]
        return 0

    lax.fori_loop(0, PAIRS, states_in, 0, unroll=2)

    a2r, a2i = cmul(ar, ai, ar, ai)
    a4r, a4i = cmul(a2r, a2i, a2r, a2i)
    a8r, a8i = cmul(a4r, a4i, a4r, a4i)

    def advance(c, carry, keep):
        vr, vi, e_all = carry
        at = pl.ds(pl.multiple_of(c * PAIRS, PAIRS), PAIRS)
        e = r.e7[at, :]
        tr, ti = (vr + r.sr[at, :]) * e, (vi + r.si[at, :]) * e
        if keep:
            r.sr[at, :], r.si[at, :] = vr, vi
        vr, vi = cmul(a8r, a8i, tr, ti)
        return vr, vi, e_all * e

    vr, vi, e_all = lax.fori_loop(0, CH, functools.partial(advance, keep=False), (zero, zero, one), unroll=8)

    at_point(0)
    causal = (iota((256, 256), 0) // 16) % Q <= (iota((256, 256), 1) // 16) % Q

    def inside(k, _):
        cr, ci = paired(r.outm[0, 2 * k], r.outm[0, 2 * k + 1]), paired(r.outm[1, 2 * k], r.outm[1, 2 * k + 1])
        qr, qi = outer(2, k, cr, ci)
        q = stacked(qr, -qi)
        r.qb[k] = q
        m = lax.dot_general(r.pb[k], q, NT, preferred_element_type=F32)
        m = jnp.where(causal, m, 0.0).astype(BF16)
        out = jnp.dot(inputs_of(k), m, preferred_element_type=F32)
        r.y[2 * k] = out[:, :128]
        r.y[2 * k + 1] = out[:, 128:]
        return 0

    def inside_part(n):
        cuts = (0, 6, 12, 16)
        lax.fori_loop(cuts[n], cuts[n + 1], inside, 0, unroll=2)

    vr, vi = comm(ar, ai, vr, vi, e_all, inside_part)
    r.ex[...] = spread_out(jnp.exp(d))
    lax.fori_loop(0, CH, functools.partial(advance, keep=True), (vr, vi, one), unroll=8)

    def outputs(k, _):
        at = pl.ds(k, CH, stride=PAIRS)
        v = jnp.concatenate([r.sr[at, :], r.si[at, :]], axis=1).astype(BF16)
        out = lax.dot_general(v, r.qb[k], NT, preferred_element_type=F32)
        r.y[2 * k] += out[:, :128]
        r.y[2 * k + 1] += out[:, 128:]
        return 0

    lax.fori_loop(0, PAIRS, outputs, 0, unroll=2)
    at_point(1)


def finish_rows(r, q):
    rows = pl.ds(pl.multiple_of(q * 128, 128), 128)

    def turn(j, _):
        parts = block_swap([r.y[j * 8 + n, pl.ds(pl.multiple_of(q * 16, 16), 16), :] for n in range(8)])
        for n in range(8):
            r.v[j, pl.ds(q * 128 + n, 16, stride=8), :] = parts[n]
        return 0

    def close(j, _):
        lanes = pl.ds(pl.multiple_of(j * 128, 128), 128)
        mixed = r.v[j, rows, :] * r.ex[rows, lanes] + r.skip[:, lanes] * r.u[rows, lanes].astype(F32)
        r.act[rows, lanes] = jax.nn.gelu(mixed).astype(BF16)
        return 0

    lax.fori_loop(0, 4, turn, 0, unroll=2)
    lax.fori_loop(0, 4, close, 0, unroll=2)


def fold(acc, vr, vi, e, wr, wi, use):
    er, ei = cmul(wr * e, wi * e, acc[0], acc[1])
    return jnp.where(use, er + vr, acc[0]), jnp.where(use, ei + vi, acc[1]), jnp.where(use, acc[2] * e, acc[2])


def squared(w, times):
    for _ in range(times):
        w = cmul(*w, *w)
    return w


class Refs:
    def __init__(self, **named):
        self.__dict__.update(named)


MIXER_SCRATCH = dict(
    fac=pltpu.VMEM((2, PAIRS, 128), F32), pw=pltpu.VMEM((4, PAIRS * Q, 128), F32), ex=pltpu.VMEM((512, 512), F32), v=pltpu.VMEM((4, 512, 128), F32),
    e7=pltpu.VMEM((CH * PAIRS, 128), F32), z=pltpu.VMEM((32, CH, 128), F32), y=pltpu.VMEM((32, CH, 128), F32),
    pb=pltpu.VMEM((PAIRS, 256, 256), BF16), qb=pltpu.VMEM((PAIRS, 256, 256), BF16),
    sr=pltpu.VMEM((CH * PAIRS, 128), F32), si=pltpu.VMEM((CH * PAIRS, 128), F32),
)


EXCHANGE_SCRATCH = dict(
    mine=pltpu.VMEM((3, 3, PAIRS, 128), F32), got_c=pltpu.VMEM((1, 3, PAIRS, 128), F32), got_x=pltpu.VMEM((3, 3, PAIRS, 128), F32),
    got_z=pltpu.VMEM((7, 3, PAIRS, 128), F32), ssem=pltpu.SemaphoreType.DMA((11,)), rsem=pltpu.SemaphoreType.DMA((11,)),
)


def greet(groups, others):
    barrier = pltpu.get_barrier_semaphore()
    peers = [{axis: lax.rem(lax.axis_index(axis) + d, count)} for axis, count in groups for d in range(1, count)] + others
    for peer in peers:
        pl.semaphore_signal(barrier, inc=1, device_id=peer, device_id_type=MESH)
    return lambda: pl.semaphore_wait(barrier, len(peers))


def exchange(r, after_x, after_z, ar, ai, vr, vi, e, part):
    core, x, z = lax.axis_index("sp_2"), lax.axis_index("sp_1"), lax.axis_index("sp_0")

    def copies(level, axis, me, count, got, first):
        return [
            pltpu.make_async_remote_copy(
                src_ref=r.mine.at[level], dst_ref=got.at[d - 1], send_sem=r.ssem.at[first + d - 1], recv_sem=r.rsem.at[first + d - 1],
                device_id={axis: lax.rem(me + d, count)}, device_id_type=MESH,
            )
            for d in range(1, count)
        ]

    def put(level, parts):
        for n, v in enumerate(parts):
            r.mine[level, n] = v

    def of(got, slot):
        return got[slot, 0], got[slot, 1], got[slot, 2]

    nothing = (jnp.zeros_like(vr), jnp.zeros_like(vr), jnp.ones_like(vr))
    w1 = squared((ar, ai), 9)
    w2 = squared(w1, 1)
    w8 = squared(w2, 2)
    own = (vr, vi, e)
    put(0, own)
    for c in copies(0, "sp_2", core, 2, r.got_c, 0):
        c.start()
    part(0)
    for c in copies(0, "sp_2", core, 2, r.got_c, 0):
        c.wait()
    other = of(r.got_c, 0)
    early = [jnp.where(core == 0, a, b) for a, b in zip(own, other)]
    late = [jnp.where(core == 0, b, a) for a, b in zip(own, other)]
    chip = fold(early, *late, *w1, True)
    put(1, chip)
    for c in copies(1, "sp_1", x, 4, r.got_x, 1):
        c.start()
    after_x()
    part(1)
    for c in copies(1, "sp_1", x, 4, r.got_x, 1):
        c.wait()
    total = nothing
    for d in (3, 2, 1):
        total = fold(total, *of(r.got_x, d - 1), *w2, d <= x)
    total = fold(total, *chip, *w2, True)
    for d in (3, 2, 1):
        total = fold(total, *of(r.got_x, d - 1), *w2, d > x)
    put(2, total)
    sends = copies(2, "sp_0", z, 8, r.got_z, 4)
    for d in range(1, 8):
        pl.when(z + d < 8)(sends[d - 1].start)
    after_z()
    part(2)
    for d in range(1, 8):
        pl.when(z + d < 8)(sends[d - 1].wait_send)
        pl.when(z >= d)(sends[d - 1].wait_recv)
    enter = nothing
    for d in range(7, 0, -1):
        enter = fold(enter, *of(r.got_z, d - 1), *w8, d <= z)
    for d in (3, 2, 1):
        enter = fold(enter, *of(r.got_x, d - 1), *w2, d <= x)
    enter = fold(enter, *other, *w1, core == 1)
    return enter[0], enter[1]

class Ring:
    def __init__(self, axis, count, many, chunk, ssem, rsem, swap=False, shared=None):
        self.axis, self.count, self.many, self.chunk, self.ssem, self.rsem = axis, count, many, chunk, ssem, rsem
        self.swap, self.shared = swap, shared
        self.me, self.half = lax.axis_index(axis), count // 2

    def place(self, steps):
        return lax.rem(self.me + steps + self.count, self.count)

    def moves(self, step, i):
        for way in (0, 1):
            j = i ^ way if self.swap else i
            if step < self.half or (step == self.half and j % 2 == way):
                yield way, j

    def copy(self, step, way, j, owner):
        n = ((step - 1) * 2 + way) * self.many + j
        ref = self.chunk(self.place(owner), j)
        return pltpu.make_async_remote_copy(
            src_ref=ref, dst_ref=ref, send_sem=self.ssem.at[n], recv_sem=self.rsem.at[n],
            device_id={self.axis: self.place(1 - 2 * way)}, device_id_type=MESH,
        )

    def partner_copy(self, step, way, j, core):
        n = ((step - 1) * 2 + way) * self.many + j
        ref = self.chunk(self.place((2 * way - 1) * step), j, core)
        return pltpu.make_async_remote_copy(
            src_ref=ref, dst_ref=ref, send_sem=self.shared[0].at[n], recv_sem=self.shared[1].at[n],
            device_id={"sp_2": 1 - lax.axis_index("sp_2")}, device_id_type=MESH,
        )

    def start(self, i):
        for way, j in self.moves(1, i):
            self.copy(1, way, j, 0).start()

    def service(self, step, i):
        onward = list(self.moves(step + 1, i))
        for way, j in self.moves(step, i):
            self.copy(step, way, j, (2 * way - 1) * step).wait_recv()
            if (way, j) in onward:
                self.copy(step + 1, way, j, (2 * way - 1) * step).start()
            if self.shared:
                self.partner_copy(step, way, j, lax.axis_index("sp_2")).start()

    def all_moves(self):
        return [(s, way, j) for s in range(1, self.half + 1) for i in range(self.many) for way, j in self.moves(s, i)]

    def shared_wait(self):
        for s, way, j in self.all_moves():
            self.partner_copy(s, way, j, 1 - lax.axis_index("sp_2")).wait_recv()

    def drain(self):
        for s, way, j in self.all_moves():
            self.copy(s, way, j, (2 * way - 1) * (s - 1)).wait_send()
            if self.shared:
                self.partner_copy(s, way, j, lax.axis_index("sp_2")).wait_send()


class RowSum:
    def __init__(self, r, n, prepare, product):
        self.part, self.far, self.near, self.own = r.part.at[n], r.far.at[n], r.near.at[n], r.own
        self.ssem, self.rsem, self.y = r.sum_s.at[n], r.sum_r.at[n], lax.axis_index("tp")
        self.prepare, self.product = prepare, product
        part, far, near = self.part, self.far, self.near
        self.copies = [
            self.copy(0, part.at[0, 0], far.at[0], 1), self.copy(1, part.at[0, 1], far.at[1], 3),
            self.copy(2, part.at[1, 1], near.at[0, 1], 1), self.copy(3, part.at[2, 0], near.at[1, 0], 3),
            self.copy(4, part.at[1, 0], near.at[0, 0], 1), self.copy(5, part.at[2, 1], near.at[1, 1], 3),
        ]

    def copy(self, n, src, dst, d):
        return pltpu.make_async_remote_copy(
            src_ref=src, dst_ref=dst, send_sem=self.ssem.at[n], recv_sem=self.rsem.at[n],
            device_id={"tp": lax.rem(self.y + d, 4)}, device_id_type=MESH,
        )

    def others(self, busy):
        for slot, d in enumerate((2, 1, 3)):
            block = lax.rem(self.y + d, 4)

            def put(side, cols, v):
                self.part[slot, side, :, cols] = v.astype(BF16)

            self.prepare(block)
            self.product(block, put)
            for c in ((0, 1), (2,), (3,))[slot]:
                self.copies[c].start()
            busy(slot)

    def mine(self):
        def put(side, cols, v):
            self.own[side, :, cols] = v

        self.prepare(self.y)
        self.product(self.y, put)

    def pass_on(self):
        for n, slot, side in ((0, 1, 0), (1, 2, 1)):
            self.copies[n].wait_recv()
            self.part[slot, side] = (self.part[slot, side].astype(F32) + self.far[n].astype(F32)).astype(BF16)
            self.copies[4 + n].start()

    def arrived(self):
        for c in self.copies[2:]:
            c.wait_recv()

    def total(self, side, cols):
        return self.own[side, :, cols] + self.near[0, side, :, cols].astype(F32) + self.near[1, side, :, cols].astype(F32)

    def drain(self):
        for c in self.copies:
            c.wait_send()


def sems(n):
    return pltpu.SemaphoreType.DMA((n,))


LAYER_SCRATCH = dict(
    act=pltpu.VMEM((512, 512), BF16), g=pltpu.VMEM((3, 8, 4, 2, 32, 1408), BF16), load=sems(3),
    stream=pltpu.VMEM((128, 2048), BF16), normed=pltpu.VMEM((33, 16, 2048), BF16),
    pre=pltpu.VMEM((2, 528, 1408), BF16), hidden=pltpu.VMEM((128, 1408), BF16),
    part=pltpu.VMEM((2, 3, 2, 128, 1024), BF16), own=pltpu.VMEM((2, 128, 1024), F32),
    far=pltpu.VMEM((2, 2, 128, 1024), BF16), near=pltpu.VMEM((2, 2, 2, 128, 1024), BF16),
    ax_s=sems(8), ax_r=sems(8), bz_s=sems(16), bz_r=sems(16), az_s=sems(32), az_r=sems(32), bx_s=sems(32), bx_r=sems(32),
    ny_s=sems(8), ny_r=sems(8), azp_s=sems(32), azp_r=sems(32), bxp_s=sems(32), bxp_r=sems(32),
    half_s=sems(2), half_r=sems(2), halo_s=sems(4), halo_r=sems(1),
    sum_s=pltpu.SemaphoreType.DMA((2, 6)), sum_r=pltpu.SemaphoreType.DMA((2, 6)),
)
SCRATCH = {**MIXER_SCRATCH, **EXCHANGE_SCRATCH, **LAYER_SCRATCH}
IN_VMEM = ("u", "damp", "ls", "rr", "ri", "inm", "outm", "skip", "residual", "gain", "taps", "w_out")
IN_HBM = ("w_act", "w_lin", "w_dn")


def layer_kernel(*refs):
    names = (*IN_VMEM, *IN_HBM, "out", *SCRATCH)
    r = Refs(**dict(zip(names, refs)))
    core, x, z, y = (lax.axis_index(a) for a in ("sp_2", "sp_1", "sp_0", "tp"))
    loads = [pltpu.make_async_copy(w, r.g.at[m, z, x, core], r.load.at[m]) for m, w in enumerate((r.w_act, r.w_lin, r.w_dn))]
    for c in loads:
        c.start()
    r.got_z[...] = jnp.zeros_like(r.got_z)
    at = z * 8 + x * 2 + core

    @pl.when(at == 0)
    def _():
        r.normed[0] = jnp.zeros((16, 2048), BF16)

    def position(n, tp):
        n = lax.rem(n, 64)
        return {"sp_0": n // 8, "sp_1": lax.rem(n, 8) // 2, "sp_2": lax.rem(n, 2), "tp": tp}

    beside = [position(at + n, q) for n in (1, 63) for q in range(4)]
    wait_for_all = greet((("sp_2", 2), ("sp_1", 4), ("sp_0", 8), ("tp", 4)), beside)

    a_cols, b_cols = pl.ds(0, 640), pl.ds(640, 768)
    a_half, b_half = (pl.ds(0, 384), pl.ds(384, 256)), (pl.ds(640, 384), pl.ds(1024, 384))
    beside_x = [lax.rem(x + n, 4) for n in (0, 1, 3, 2)]
    beside_z = [lax.rem(z + n, 8) for n in (0, 1, 7, 2, 6, 3, 5, 4)]
    ax = Ring("sp_1", 4, 2, lambda o, j: r.g.at[:, z, o, core, :, a_half[j]], r.ax_s, r.ax_r, True)
    bz = Ring("sp_0", 8, 2, lambda o, j: r.g.at[:, o, x, core, :, b_half[j]], r.bz_s, r.bz_r, True)
    az = Ring("sp_0", 8, 4, lambda o, j, c=core: r.g.at[:, o, beside_x[j], c, :, a_cols], r.az_s, r.az_r, False, (r.azp_s, r.azp_r))
    bx = Ring("sp_1", 4, 8, lambda o, j, c=core: r.g.at[:, beside_z[j], o, c, :, b_cols], r.bx_s, r.bx_r, False, (r.bxp_s, r.bxp_r))
    ny = Ring("tp", 4, 2, lambda o, j: r.normed.at[pl.ds(1 + o * 8 + j * 4, 4)], r.ny_s, r.ny_r, True)

    def half_copies(c):
        return [
            pltpu.make_async_remote_copy(
                src_ref=ref, dst_ref=ref, send_sem=r.half_s.at[n], recv_sem=r.half_r.at[n], device_id={"sp_2": 1 - core}, device_id_type=MESH
            )
            for n, ref in enumerate((r.g.at[:, z, :, c, :, a_cols], r.g.at[:, :, x, c, :, b_cols]))
        ]

    def serve(*steps):
        for ring, step, i in steps:
            ring.service(step, i)

    def greeted():
        for c in loads:
            c.wait()
        wait_for_all()
        for i in (0, 1):
            ax.start(i)
            bz.start(i)
        bx.start(0)
        az.start(0)

    def at_point(n):
        if n == 0:
            serve((ax, 1, 0), (ax, 1, 1), (bz, 1, 0), (bz, 1, 1))
        else:
            serve((az, 1, 1))

    def after_x():
        az.start(1)
        bx.start(1)
        bx.start(2)

    def after_z():
        az.start(2)
        serve((bz, 2, 0), (bz, 2, 1), (ax, 2, 0))
        az.start(3)
        serve((az, 1, 0))
        bx.start(3)
        bx.start(4)
        serve((bx, 1, 0))

    mixer_phase(r, greeted, functools.partial(exchange, r, after_x, after_z), at_point)

    def project(b, put):
        rows = pl.ds(pl.multiple_of(b * 128, 128), 128)

        def tile(n, _):
            cols = pl.ds(pl.multiple_of(n * 512, 512), 512)
            v = jnp.dot(r.act[rows, :], r.w_out[:, cols], preferred_element_type=F32)
            put(n // 2, pl.ds(pl.multiple_of((n % 2) * 512, 512), 512), v)
            return 0

        lax.fori_loop(0, 4, tile, 0)

    def while_projecting(slot):
        if slot == 2:
            serve((az, 1, 2), (bx, 1, 1), (bx, 1, 2))

    first = RowSum(r, 0, functools.partial(finish_rows, r), project)
    first.others(while_projecting)
    first.mine()
    serve((bz, 3, 0), (bz, 3, 1))
    bx.start(5)
    bx.start(6)
    first.pass_on()
    serve((az, 1, 3), (bx, 1, 3), (az, 2, 0), (bx, 1, 4), (bz, 4, 0))
    bx.start(7)
    for c in half_copies(core):
        c.start()
    serve((az, 2, 1), (bx, 1, 5), (az, 2, 2))
    first.arrived()

    def add_up(n, squares):
        cols = pl.ds(pl.multiple_of(n * 256, 256), 256)
        total = r.residual[:, cols].astype(F32) + first.total(n // 4, pl.ds(pl.multiple_of((n % 4) * 256, 256), 256))
        total = total.astype(BF16)
        r.stream[:, cols] = total
        total = total.astype(F32)
        return squares + total * total

    squares = lax.fori_loop(0, 8, add_up, jnp.zeros((128, 256), F32))
    scale = lax.rsqrt(jnp.sum(squares, axis=1, keepdims=True) / 2048 + 1e-06)

    def normalize(n, _):
        cols = pl.ds(pl.multiple_of(n * 256, 256), 256)
        v = (r.stream[:, cols].astype(F32) * scale * r.gain[:, cols]).astype(BF16)
        r.normed[pl.ds(1 + 8 * y, 8), :, cols] = v.reshape(8, 16, 256)
        return 0

    lax.fori_loop(0, 8, normalize, 0)
    ny.start(0)
    ny.start(1)
    halos = [
        pltpu.make_async_remote_copy(
            src_ref=r.normed.at[32], dst_ref=r.normed.at[0], send_sem=r.halo_s.at[q], recv_sem=r.halo_r.at[0],
            device_id=position(at + 1, q), device_id_type=MESH,
        )
        for q in range(4)
    ]
    ends = jnp.logical_and(y == 3, at < 63)

    @pl.when(ends)
    def _():
        for c in halos:
            c.start()

    serve((az, 2, 3), (bx, 1, 6), (az, 3, 0), (bx, 1, 7), (az, 3, 1), (az, 3, 2), (ny, 1, 0), (az, 3, 3))
    serve(*((bx, 2, j) for j in range(8)))
    serve((az, 4, 0), (az, 4, 1), (ny, 1, 1), (az, 4, 2), (az, 4, 3))
    for c in half_copies(1 - core):
        c.wait_recv()
    bx.shared_wait()
    az.shared_wait()
    pl.when(at > 0)(halos[0].wait_recv)
    serve((ny, 2, 0))

    def up(w, m, cols):
        out = jnp.dot(r.normed[...].reshape(528, 2048), w, preferred_element_type=F32)
        r.pre[m, :, cols] = out.astype(BF16)

    def up_tile(b, _):
        cols = pl.ds(pl.multiple_of((b // 2) * 256, 256), 256)
        up(r.g[b % 2, :, :, :, :, cols].reshape(2048, 256), b % 2, cols)
        return 0

    lax.fori_loop(0, 10, up_tile, 0)
    tail = pl.ds(1280, 128)
    w = jnp.concatenate([r.g[m, :, :, :, :, tail].reshape(2048, 128) for m in (0, 1)], axis=1)
    out = jnp.dot(r.normed[...].reshape(528, 2048), w, preferred_element_type=F32).astype(BF16)
    r.pre[0, :, tail], r.pre[1, :, tail] = out[:, :128], out[:, 128:]

    def convolved(b, m, cols):
        v = r.pre[m, pl.ds(pl.multiple_of(b * 128, 128), 144), cols].astype(F32)
        return sum(r.taps[k, pl.ds(m, 1), cols] * v[14 + k : 142 + k] for k in range(3))

    def hide(b):
        def tile(n, _):
            cols = pl.ds(pl.multiple_of(n * 128, 128), 128)
            a, l = convolved(b, 0, cols), convolved(b, 1, cols)
            r.hidden[:, cols] = (a / (1.0 + jnp.exp(-a)) * l).astype(BF16)
            return 0

        lax.fori_loop(0, 11, tile, 0)

    def down(b, put):
        def tile(n, _):
            w = r.g[2, pl.ds(n, 1)].reshape(256, 1408)
            put(n // 4, pl.ds(pl.multiple_of((n % 4) * 256, 256), 256), lax.dot_general(r.hidden[...], w, NT, preferred_element_type=F32))
            return 0

        lax.fori_loop(0, 8, tile, 0)

    second = RowSum(r, 1, hide, down)
    second.others(lambda slot: None)
    second.pass_on()
    second.mine()
    second.arrived()

    def close(n, _):
        cols = pl.ds(pl.multiple_of(n * 256, 256), 256)
        total = second.total(n // 4, pl.ds(pl.multiple_of((n % 4) * 256, 256), 256))
        r.out[:, cols] = (r.stream[:, cols].astype(F32) + total).astype(BF16)
        return 0

    lax.fori_loop(0, 8, close, 0, unroll=2)
    for ring in (ax, bz, az, bx, ny):
        ring.drain()
    for c in half_copies(core):
        c.wait_send()
    first.drain()
    second.drain()

    @pl.when(ends)
    def _():
        for c in halos:
            c.wait_send()


def per_device(
    mixer_input, residual, log_step, rate_real, rate_imag, damping, in_map, out_map, skip, w_out, norm_gain, w_act, w_lin, conv_taps, w_down
):
    in_vmem = (
        mixer_input, damping.T, jnp.broadcast_to(log_step[:, None], rate_real.shape), rate_real, rate_imag,
        in_map.transpose(0, 1, 3, 2), out_map, skip[None], residual, norm_gain[None], conv_taps.transpose(1, 0, 2), w_out,
    )
    in_hbm = (w_act, w_lin, w_down.T)
    return pl.pallas_call(
        layer_kernel,
        out_shape=jax.ShapeDtypeStruct(residual.shape, BF16),
        in_specs=[pl.BlockSpec(memory_space=pltpu.VMEM)] * len(in_vmem) + [pl.BlockSpec(memory_space=pl.ANY)] * len(in_hbm),
        out_specs=pl.BlockSpec(memory_space=pltpu.VMEM),
        scratch_shapes=list(SCRATCH.values()),
        compiler_params=pltpu.CompilerParams(collective_id=0, has_side_effects=True, vmem_limit_bytes=60 * 2**20),
        name="layer",
    )(*in_vmem, *in_hbm)


def solution(mesh):
    split = Mesh(mesh.devices.reshape(8, 4, 2, mesh.shape["tp"]), ("sp_0", "sp_1", "sp_2", "tp"))
    in_specs = (
        P(SP, "tp"),
        P(SP_TP, None),
        P("tp"),
        P("tp", None),
        P("tp", None),
        P(SP, "tp"),
        P(None, "tp", None, None),
        P(None, "tp", None, None),
        P("tp"),
        P("tp", None),
        P(),
        P(SP, "tp"),
        P(SP, "tp"),
        P(None, None, "tp"),
        P("tp", SP),
    )
    out_specs = P(SP_TP, None)
    return jax.shard_map(
        per_device, mesh=split, in_specs=in_specs, out_specs=out_specs, check_vma=False
    )
```

time: 233 us -> 108 us (0.46)
  waiting for transfers between devices: 67.1 us -> 0 us
  Pallas kernels: 39.6 us -> 102 us
  blocking collectives: 56.8 us -> 0 us
  matrix products: 25.8 us -> 0 us
  between operations: 13.6 us -> 0.01 us
  starting transfers between devices: 13.5 us -> 0 us
  other arithmetic: 7.69 us -> 0 us
  local copies, waits for them, and re-layouts: 8.55 us -> 3.21 us
    pallas_call x1, Pallas kernels: 39.6 us -> 102 us  [per_device(): pl.pallas_call(layer_kernel, out_shape=jax.ShapeDtypeStruct(residual.shap...]
    all_to_all x2 -> x0, blocking collectives: 56.8 us -> none  [sent_and_summed(): lax.all_to_all(parts, axis, split_axis=0, concat_axis=0, tiled=True)]
    all_gather x2 -> x0, waiting for transfers between devices: 44.7 us -> none  [the longest x1 44.7 us: per_device(): down_full = lax.all_gather(w_down, SP, axis=1, tiled=True)]
    dot_general x4 -> x0, matrix products: 25.8 us -> none  [the longest x1 12.6 us: per_device(): jnp.dot(block, down_full, preferred_element_type=jnp.float32)]
    all_to_all x1 -> x0, waiting for transfers between devices: 21.8 us -> none  [from_everyone(): return lax.all_to_all(copies, axis, split_axis=0, concat_axis=0, tiled=True)]
    ppermute x2 -> x0, starting transfers between devices: 8.98 us -> none  [from_behind(): lax.ppermute(value, axis, [(source, source + steps) for source in range(i...]
    convert_element_type x4 -> x0, other arithmetic: 4.91 us -> none  [the longest x1 1.93 us: causal_conv(): jnp.concatenate([previous[0], act_pre], axis=0).astype(jnp.float32)]
    all_to_all x1 -> x0, starting transfers between devices: 4.46 us -> none  [from_everyone(): return lax.all_to_all(copies, axis, split_axis=0, concat_axis=0, tiled=True)]
  transfers between devices with their start and end apart: 5 -> 0, of which waited for: 2 -> 0; matrix products, arithmetic and copies ran while one was open for 9% -> 0% of each run, Pallas kernels for 17% -> 0%
where the time goes in v2:
time: 108 us; the launch traced here: 106 us
  Pallas kernels  102 us (94%)
  local copies, waits for them, and re-layouts  3.21 us (3%)
    pallas_call x1, Pallas kernels, per_device(): pl.pallas_call(layer_kernel, out_shape=jax.ShapeDtypeStruct(residual.shap...  102 us

profile of v2, /device:TPU:1, one launch (start us, length us, event | category | flops | bytes accessed | tf_op | source)
XLA Modules:
  0.0 105.7 jit_solution(16203521798478510672)
XLA Ops:
  0.0 1.3 %broadcast_in_dim.12.refs_2_ = f32[32,64]{1,0:T(8,128)} broadcast(f32[32]{0:T(128)} %param.17), dimensions={0} | broadcast | bytes 8320 | tf_op jit(solution)/shard_map/broadcast_in_dim | solution.py:650
  1.3 102.5 %layer.1 = bf16[128,2048]{1,0:T(8,128)(2,1)} custom-call(bf16[512,512]{1,0:T(8,128)(2,1)} %refs_0_.1, f32[32,512]{1,0:T(8,128)} %bitcast.8, f32[32,64]{1,0:T(8,128)} %broadcast_in_dim.12.refs_2_, f32[32,64]{1,0:T(8,128)} %refs_3_.1, f32[32,64]{1,0:T(8,128)} %refs_4_.1, f32[2,32,16,64]{3,2,1,0:T(8,128)} %bitcast.6, f32[2,32,16,64]{3,2,1,0:T(8,128)} %refs_6_.1, ...), custom_call_target="tpu_custom_call" | custom-call | tf_op jit(solution)/shard_map/layer/pallas_call | solution.py:654
  103.8 1.9 %copy.17 = bf16[128,2048]{1,0:T(8,128)(2,1)} copy(bf16[128,2048]{1,0:T(8,128)(2,1)} %layer.1) | data formatting | bytes 1048576

commit v3 on v2

v3 whole, which is shorter than its diff:
```python
import functools

import jax
import jax.numpy as jnp
from jax import lax
from jax.experimental import pallas as pl
from jax.experimental.pallas import tpu as pltpu
from jax.sharding import Mesh
from jax.sharding import PartitionSpec as P

F32, BF16 = jnp.float32, jnp.bfloat16
NT = (((1,), (1,)), ((), ()))
TN = (((0,), (0,)), ((), ()))
Q, CH, PAIRS = 8, 64, 16
SP = ("sp_0", "sp_1", "sp_2")
SP_TP = ("sp_0", "sp_1", "sp_2", "tp")
MESH = pl.DeviceIdType.MESH

def iota(shape, dim):
    return lax.broadcasted_iota(jnp.int32, shape, dim)

def cmul(ar, ai, br, bi):
    return ar * br - ai * bi, ar * bi + ai * br

def split3(x):
    hi = x.astype(BF16)
    r = x - hi.astype(F32)
    mid = r.astype(BF16)
    lo = (r - mid.astype(F32)).astype(BF16)
    return hi, mid, lo

def block_swap(parts):
    parts = list(parts)
    block = iota(parts[0].shape, 1) // 16
    for b in (4, 2, 1):
        here = (block // b) % 2 == 0
        for n in range(8):
            if n & b == 0:
                low, high = parts[n], parts[n + b]
                parts[n] = jnp.where(here, low, pltpu.roll(high, 16 * b, axis=1))
                parts[n + b] = jnp.where(here, pltpu.roll(low, 128 - 16 * b, axis=1), high)
    return parts


def paired(even, odd):
    return jnp.concatenate([even, odd], axis=1)


def mixer_phase(r, greeted, comm):
    def rows(ref):
        return paired(ref[pl.ds(0, PAIRS, stride=2), :], ref[pl.ds(1, PAIRS, stride=2), :])

    square = iota((32, 32), 0) == iota((32, 32), 1)
    r.steps[...] = jnp.broadcast_to(jnp.sum(jnp.where(square, r.ls[...], 0.0), axis=1, keepdims=True), (32, 64))
    rr, ri = rows(r.rr), rows(r.ri)
    step = jnp.exp(rows(r.steps))
    lr, th = rr * step, ri * step
    cos, sin = jnp.cos(th), jnp.sin(th)
    mag, inv = jnp.exp(lr), jnp.exp(-lr)
    ar, ai = mag * cos, mag * sin
    den = rr * rr + ri * ri
    r.fac[0] = ((ar - 1.0) * rr + ai * ri) / den
    r.fac[1] = (ai * rr - (ar - 1.0) * ri) / den
    one, zero = jnp.ones_like(ar), jnp.zeros_like(ar)
    pr, pi, nr, ni = one, zero, one, zero
    for s in range(Q):
        at = pl.ds(s, PAIRS, stride=Q)
        r.pw[0, at, :], r.pw[1, at, :] = nr, ni
        r.pw[2, at, :], r.pw[3, at, :] = pr, pi
        pr, pi = cmul(pr, pi, ar, ai)
        nr, ni = cmul(nr, ni, inv * cos, -inv * sin)
    d = r.damp[...]
    lane = iota(d.shape, 1) % Q
    for sh in (1, 2, 4):
        d = d + jnp.where(lane >= sh, pltpu.roll(d, sh, axis=1), 0.0)
    ex = (iota((96, 512), 0) % 32 == iota((96, 512), 1) // 16).astype(F32).astype(BF16)
    def spread_out(v):
        parts = jnp.concatenate([p.astype(F32) for p in split3(v)], axis=0).astype(BF16)
        return lax.dot_general(parts, ex, TN, preferred_element_type=F32)

    pick = (iota((CH, 512), 1) == Q * iota((CH, 512), 0) + Q - 1).astype(F32).astype(BF16)
    ends = sum(lax.dot_general(pick, p, NT, preferred_element_type=F32) for p in split3(d))
    ends = jnp.exp(ends)
    low = iota((CH, 128), 1) < 64
    for k in range(PAIRS):
        r.e7[pl.ds(k, CH, stride=PAIRS), :] = jnp.where(low, ends[:, 2 * k : 2 * k + 1], ends[:, 2 * k + 1 : 2 * k + 2])

    r.ex[...] = spread_out(jnp.exp(d))
    shrink = spread_out(jnp.exp(-d)) * r.u[...].astype(F32)
    for j in range(4):
        r.v[j] = shrink[:, j * 128 : j * 128 + 128]

    def spread(b, _):
        j, c = b // 2, b % 2
        parts = block_swap([r.v[j, pl.ds(c * 256 + n, 32, stride=8), :] for n in range(8)])
        for n in range(8):
            r.z[j * 8 + n, pl.ds(pl.multiple_of(c * 32, 32), 32), :] = parts[n]
        return 0

    lax.fori_loop(0, 8, spread, 0)
    greeted()

    low = iota((128, 128), 1) < 64

    def stacked(re, im):
        top = jnp.concatenate([jnp.where(low, re, 0.0), jnp.where(low, im, 0.0)], axis=1)
        bottom = jnp.concatenate([jnp.where(low, 0.0, re), jnp.where(low, 0.0, im)], axis=1)
        return jnp.concatenate([top, bottom], axis=0).astype(BF16)

    def outer(which, k, br, bi):
        at = pl.ds(pl.multiple_of(k * Q, Q), Q)
        wr, wi = r.pw[which, at, :][:, None, :], r.pw[which + 1, at, :][:, None, :]
        br, bi = br[None], bi[None]
        re, im = cmul(wr, wi, br, bi)
        return re.reshape(128, 128), im.reshape(128, 128)

    def inputs_of(k):
        return jnp.concatenate([r.z[2 * k], r.z[2 * k + 1]], axis=1).astype(BF16)

    def states_in(k, _):
        br, bi = paired(r.inm[0, 2 * k], r.inm[0, 2 * k + 1]), paired(r.inm[1, 2 * k], r.inm[1, 2 * k + 1])
        br, bi = cmul(r.fac[0, pl.ds(k, 1), :], r.fac[1, pl.ds(k, 1), :], br, bi)
        p = stacked(*outer(0, k, br, bi))
        r.pb[k] = p
        s = jnp.dot(inputs_of(k), p, preferred_element_type=F32)
        at = pl.ds(k, CH, stride=PAIRS)
        r.sr[at, :] = s[:, :128]
        r.si[at, :] = s[:, 128:]
        return 0

    lax.fori_loop(0, PAIRS, states_in, 0, unroll=2)

    a2r, a2i = cmul(ar, ai, ar, ai)
    a4r, a4i = cmul(a2r, a2i, a2r, a2i)
    a8r, a8i = cmul(a4r, a4i, a4r, a4i)

    def advance(c, carry, keep):
        vr, vi, e_all = carry
        at = pl.ds(pl.multiple_of(c * PAIRS, PAIRS), PAIRS)
        e = r.e7[at, :]
        tr, ti = (vr + r.sr[at, :]) * e, (vi + r.si[at, :]) * e
        if keep:
            r.sr[at, :], r.si[at, :] = vr, vi
        vr, vi = cmul(a8r, a8i, tr, ti)
        return vr, vi, e_all * e

    vr, vi, e_all = lax.fori_loop(0, CH, functools.partial(advance, keep=False), (zero, zero, one), unroll=8)

    causal = (iota((256, 256), 0) // 16) % Q <= (iota((256, 256), 1) // 16) % Q

    def inside(k, _):
        cr, ci = paired(r.outm[0, 2 * k], r.outm[0, 2 * k + 1]), paired(r.outm[1, 2 * k], r.outm[1, 2 * k + 1])
        qr, qi = outer(2, k, cr, ci)
        q = stacked(qr, -qi)
        r.qb[k] = q
        m = lax.dot_general(r.pb[k], q, NT, preferred_element_type=F32)
        m = jnp.where(causal, m, 0.0).astype(BF16)
        out = jnp.dot(inputs_of(k), m, preferred_element_type=F32)
        r.y[2 * k] = out[:, :128]
        r.y[2 * k + 1] = out[:, 128:]
        return 0

    def inside_part(n):
        cuts = (0, 10, 16)
        lax.fori_loop(cuts[n], cuts[n + 1], inside, 0, unroll=2)

    vr, vi = comm(ar, ai, vr, vi, e_all, inside_part)
    lax.fori_loop(0, CH, functools.partial(advance, keep=True), (vr, vi, one), unroll=8)

    def outputs(k, _):
        at = pl.ds(k, CH, stride=PAIRS)
        v = jnp.concatenate([r.sr[at, :], r.si[at, :]], axis=1).astype(BF16)
        out = lax.dot_general(v, r.qb[k], NT, preferred_element_type=F32)
        r.y[2 * k] += out[:, :128]
        r.y[2 * k + 1] += out[:, 128:]
        return 0

    lax.fori_loop(0, PAIRS, outputs, 0, unroll=2)


def finish_rows(r, q, slot):
    rows = pl.ds(pl.multiple_of(q * 128, 128), 128)

    def turn(j, _):
        parts = block_swap([r.y[j * 8 + n, pl.ds(pl.multiple_of(q * 16, 16), 16), :] for n in range(8)])
        for n in range(8):
            r.v[j, pl.ds(q * 128 + n, 16, stride=8), :] = parts[n]
        return 0

    def close(j, _):
        lanes = pl.ds(pl.multiple_of(j * 128, 128), 128)
        mixed = r.v[j, rows, :] * r.ex[rows, lanes] + r.skip[:, lanes] * r.u[rows, lanes].astype(F32)
        r.act[rows, lanes] = jax.nn.gelu(mixed).astype(BF16)
        return 0

    lax.fori_loop(0, 4, turn, 0, unroll=2)
    lax.fori_loop(0, 4, close, 0, unroll=2)


def fold(acc, vr, vi, e, wr, wi, use):
    er, ei = cmul(wr * e, wi * e, acc[0], acc[1])
    return jnp.where(use, er + vr, acc[0]), jnp.where(use, ei + vi, acc[1]), jnp.where(use, acc[2] * e, acc[2])


def squared(w, times):
    for _ in range(times):
        w = cmul(*w, *w)
    return w


class Refs:
    def __init__(self, **named):
        self.__dict__.update(named)


MIXER_SCRATCH = dict(
    steps=pltpu.VMEM((32, 64), F32), fac=pltpu.VMEM((2, PAIRS, 128), F32), pw=pltpu.VMEM((4, PAIRS * Q, 128), F32), ex=pltpu.VMEM((512, 512), F32), v=pltpu.VMEM((4, 512, 128), F32),
    e7=pltpu.VMEM((CH * PAIRS, 128), F32), z=pltpu.VMEM((32, CH, 128), F32), y=pltpu.VMEM((32, CH, 128), F32),
    pb=pltpu.VMEM((PAIRS, 256, 256), BF16), qb=pltpu.VMEM((PAIRS, 256, 256), BF16),
    sr=pltpu.VMEM((CH * PAIRS, 128), F32), si=pltpu.VMEM((CH * PAIRS, 128), F32),
)


EXCHANGE_SCRATCH = dict(
    mine=pltpu.VMEM((2, 3, PAIRS, 128), F32), got_p=pltpu.VMEM((7, 3, PAIRS, 128), F32),
    got_z=pltpu.VMEM((7, 3, PAIRS, 128), F32), ssem=pltpu.SemaphoreType.DMA((14,)), rsem=pltpu.SemaphoreType.DMA((14,)),
)


def in_plane(n):
    n = lax.rem(n, 8)
    return {"sp_1": n // 2, "sp_2": lax.rem(n, 2)}


def greet(peers):
    barrier = pltpu.get_barrier_semaphore()
    for peer in peers:
        pl.semaphore_signal(barrier, inc=1, device_id=peer, device_id_type=MESH)
    return lambda: pl.semaphore_wait(barrier, len(peers))


def exchange(r, after_own, after_inside, after_plane, after_z, ar, ai, vr, vi, e, part):
    at, z = lax.axis_index("sp_1") * 2 + lax.axis_index("sp_2"), lax.axis_index("sp_0")

    def copy(level, d, got, peer):
        n = level * 7 + d - 1
        return pltpu.make_async_remote_copy(
            src_ref=r.mine.at[level], dst_ref=got.at[d - 1], send_sem=r.ssem.at[n], recv_sem=r.rsem.at[n],
            device_id=peer, device_id_type=MESH,
        )

    def put(level, parts):
        for n, v in enumerate(parts):
            r.mine[level, n] = v

    def of(got, d):
        return got[d - 1, 0], got[d - 1, 1], got[d - 1, 2]

    nothing = (jnp.zeros_like(vr), jnp.zeros_like(vr), jnp.ones_like(vr))
    w1 = squared((ar, ai), 9)
    w8 = squared(w1, 3)
    own = (vr, vi, e)
    put(0, own)
    plane = [copy(0, d, r.got_p, in_plane(at + d)) for d in range(1, 8)]
    for d in (4, 3, 5, 2, 6, 1, 7):
        plane[d - 1].start()
    after_own()
    part(0)
    after_inside()
    for c in plane:
        c.wait()
    total = nothing
    for d in range(7, 0, -1):
        total = fold(total, *of(r.got_p, d), *w1, d <= at)
    total = fold(total, *own, *w1, True)
    for d in range(7, 0, -1):
        total = fold(total, *of(r.got_p, d), *w1, d > at)
    put(1, total)
    sends = [copy(1, d, r.got_z, {"sp_0": lax.rem(z + d, 8)}) for d in range(1, 8)]
    for d in range(1, 8):
        pl.when(z + d < 8)(sends[d - 1].start)
    after_plane()
    part(1)
    after_z()
    for d in range(1, 8):
        pl.when(z + d < 8)(sends[d - 1].wait_send)
        pl.when(z >= d)(sends[d - 1].wait_recv)
    enter = nothing
    for d in range(7, 0, -1):
        enter = fold(enter, *of(r.got_z, d), *w8, d <= z)
    for d in range(7, 0, -1):
        enter = fold(enter, *of(r.got_p, d), *w1, d <= at)
    return enter[0], enter[1]


class Ring:
    def __init__(self, axis, count, many, chunk, others, sent, rsem, swap=False, shared=None):
        self.axis, self.count, self.many, self.chunk, self.others, self.sent, self.rsem = axis, count, many, chunk, others, sent, rsem
        self.swap, self.shared = swap, shared
        self.me, self.half = lax.axis_index(axis), count // 2

    def place(self, steps):
        return lax.rem(self.me + steps + self.count, self.count)

    def moves(self, step, i):
        for way in (0, 1):
            j = i ^ way if self.swap else i
            if step < self.half or (step == self.half and j % 2 == way):
                yield way, j

    def copy(self, step, way, j, owner):
        n = ((step - 1) * 2 + way) * self.many + j
        ref = self.chunk(self.place(owner), j)
        return pltpu.make_async_remote_copy(
            src_ref=ref, dst_ref=ref, send_sem=self.sent, recv_sem=self.rsem.at[n],
            device_id={self.axis: self.place(1 - 2 * way)}, device_id_type=MESH,
        )

    def to_partner(self, ref):
        return pltpu.make_async_remote_copy(
            src_ref=ref, dst_ref=ref, send_sem=self.shared.at[0], recv_sem=self.shared.at[1],
            device_id={"sp_2": 1 - lax.axis_index("sp_2")}, device_id_type=MESH,
        )

    def start(self, i):
        for way, j in self.moves(1, i):
            self.copy(1, way, j, 0).start()

    def service(self, step, i):
        onward = list(self.moves(step + 1, i))
        for way, j in self.moves(step, i):
            self.copy(step, way, j, (2 * way - 1) * step).wait_recv()
            if (way, j) in onward:
                self.copy(step + 1, way, j, (2 * way - 1) * step).start()
            if self.shared is not None:
                self.to_partner(self.chunk(self.place((2 * way - 1) * step), j)).start()

    def shared_wait(self):
        self.to_partner(self.others).wait_recv()

    def drain(self):
        pltpu.make_async_remote_copy(
            src_ref=self.others, dst_ref=self.others, send_sem=self.sent, recv_sem=self.rsem.at[0],
            device_id={self.axis: self.place(1)}, device_id_type=MESH,
        ).wait_send()
        if self.shared is not None:
            self.to_partner(self.others).wait_send()


class RowSum:
    def __init__(self, part, far, near, own, sent, rsem, prepare, quarter):
        self.part, self.far, self.near, self.own, self.sent, self.rsem = part, far, near, own, sent, rsem
        self.y, self.prepare, self.quarter = lax.axis_index("tp"), prepare, quarter
        self.fars = [self.copy(n, part.at[0, n], far.at[n], 1 if n < 2 else 3) for n in range(4)]
        self.nears = [
            self.copy(4, part.at[1, pl.ds(2, 2)], near.at[0, pl.ds(2, 2)], 1), self.copy(5, part.at[2, pl.ds(0, 2)], near.at[1, pl.ds(0, 2)], 3)
        ]
        self.sums = [self.copy(6 + n, part.at[1 + n // 2, n], near.at[n // 2, n], 1 if n < 2 else 3) for n in range(4)]

    def copy(self, n, src, dst, d):
        return pltpu.make_async_remote_copy(
            src_ref=src, dst_ref=dst, send_sem=self.sent, recv_sem=self.rsem.at[n],
            device_id={"tp": lax.rem(self.y + d, 4)}, device_id_type=MESH,
        )

    def make(self, slot, d, *order):
        for n in order:
            self.part[slot, n] = self.quarter(lax.rem(self.y + d, 4), n, slot).astype(BF16)

    def others(self, busy):
        self.prepare(lax.rem(self.y + 2, 4), 0)
        for pair in ((0, 2), (1, 3)):
            self.make(0, 2, *pair)
            for n in pair:
                self.fars[n].start()
        busy(0)
        self.prepare(lax.rem(self.y + 1, 4), 1)
        self.make(1, 1, 2, 3)
        self.nears[0].start()
        busy(1)
        self.prepare(lax.rem(self.y + 3, 4), 2)
        self.make(2, 3, 0, 1)
        self.nears[1].start()
        self.make(2, 3, 2, 3)
        self.make(1, 1, 0, 1)
        busy(2)

    def mine(self):
        self.prepare(self.y, 3)
        for n in range(4):
            self.own[n] = self.quarter(self.y, n, 3)

    def pass_on(self):
        for n in (0, 2, 1, 3):
            self.fars[n].wait_recv()
            slot = 1 + n // 2
            self.part[slot, n] = (self.part[slot, n].astype(F32) + self.far[n].astype(F32)).astype(BF16)
            self.sums[n].start()

    def arrived(self):
        for c in self.nears + self.sums:
            c.wait_recv()

    def total(self, n, at):
        return self.own[n][at] + self.near[0, n][at].astype(F32) + self.near[1, n][at].astype(F32)

    def drain(self):
        self.copy(0, self.part, self.part, 1).wait_send()


def sems(n):
    return pltpu.SemaphoreType.DMA((n,))


IN_VMEM = dict(
    u=((512, 512), BF16), damp=((32, 512), F32), ls=((1, 32), F32), rr=((32, 64), F32), ri=((32, 64), F32), inm=((2, 32, 16, 64), F32),
    outm=((2, 32, 16, 64), F32), skip=((1, 512), F32), residual=((128, 2048), BF16), gain=((1, 2048), F32), taps=((3, 2, 1408), F32),
    w_out=((512, 2048), BF16),
)
EARLY = ("u", "damp", "ls", "rr", "ri", "inm", "outm", "skip")
WEIGHTS = ("w_act", "w_lin", "w_dn")
LAYER_SCRATCH = dict(
    act=pltpu.VMEM((512, 512), BF16), g=pltpu.VMEM((3, 8, 4, 2, 32, 1408), BF16), load=sems(4), result=pltpu.VMEM((128, 2048), BF16),
    stream=pltpu.VMEM((128, 2048), BF16), normed=pltpu.VMEM((33, 16, 2048), BF16),
    pre=pltpu.VMEM((2, 528, 1408), BF16), hidden=pltpu.VMEM((3, 128, 1408), BF16),
    part1=pltpu.VMEM((3, 4, 128, 512), BF16), far1=pltpu.VMEM((4, 128, 512), BF16), near1=pltpu.VMEM((2, 4, 128, 512), BF16),
    own1=pltpu.VMEM((4, 128, 512), F32), sum1_r=sems(10),
    part2=pltpu.VMEM((3, 4, 512, 128), BF16), far2=pltpu.VMEM((4, 512, 128), BF16), near2=pltpu.VMEM((2, 4, 512, 128), BF16),
    own2=pltpu.VMEM((4, 512, 128), F32), sum2_r=sems(10),
    sent=sems(7), ax_r=sems(8), bz_r=sems(16), az_r=sems(32), bx_r=sems(32), ny_r=sems(8), azp=sems(2), bxp=sems(2),
    half_s=sems(2), half_r=sems(2), halo_s=sems(4), halo_r=sems(1),
)
SCRATCH = {**MIXER_SCRATCH, **EXCHANGE_SCRATCH, **LAYER_SCRATCH}


def layer_kernel(*refs):
    given = dict(zip((*IN_VMEM, *WEIGHTS), refs))
    target = refs[len(given)]
    scratch = refs[len(given) + 1 :]
    r = Refs(**dict(zip(IN_VMEM, scratch)), **dict(zip(SCRATCH, scratch[len(IN_VMEM) :])))
    core, x, z, y = (lax.axis_index(a) for a in ("sp_2", "sp_1", "sp_0", "tp"))
    at = z * 8 + x * 2 + core

    def position(n, tp):
        n = lax.rem(n, 64)
        return {"sp_0": n // 8, "sp_1": lax.rem(n, 8) // 2, "sp_2": lax.rem(n, 2), "tp": tp}

    loads = [pltpu.make_async_copy(given[name], getattr(r, name), r.load.at[0 if name in EARLY else 1]) for name in IN_VMEM]
    weights = [pltpu.make_async_copy(given[w], r.g.at[m, z, x, core], r.load.at[2]) for m, w in enumerate(WEIGHTS)]
    for c in loads[: len(EARLY)] + weights + loads[len(EARLY) :]:
        c.start()
    r.got_z[...] = jnp.zeros_like(r.got_z)
    @pl.when(at == 0)
    def _():
        r.normed[0] = jnp.zeros((16, 2048), BF16)

    peers = [in_plane(x * 2 + core + d) for d in range(1, 8)]
    peers += [{axis: lax.rem(lax.axis_index(axis) + d, count)} for axis, count in (("sp_0", 8), ("tp", 4)) for d in range(1, count)]
    peers += [position(at + n, q) for n in (1, 63) for q in range(4)]
    wait_for_all = greet(peers)
    for c in loads[: len(EARLY)]:
        c.wait()

    a_cols, b_cols = pl.ds(0, 640), pl.ds(640, 768)
    a_half, b_half = (pl.ds(0, 384), pl.ds(384, 256)), (pl.ds(640, 384), pl.ds(1024, 384))
    beside_x = [lax.rem(x + n, 4) for n in (0, 1, 3, 2)]
    beside_z = [lax.rem(z + n, 8) for n in (0, 1, 7, 2, 6, 3, 5, 4)]
    ax = Ring("sp_1", 4, 2, lambda o, j: r.g.at[:, z, o, core, :, a_half[j]], r.g.at[:, z, pl.ds(0, 3), core, :, a_cols], r.sent.at[0], r.ax_r, True)
    bz = Ring("sp_0", 8, 2, lambda o, j: r.g.at[:, o, x, core, :, b_half[j]], r.g.at[:, pl.ds(0, 7), x, core, :, b_cols], r.sent.at[1], r.bz_r, True)
    az = Ring("sp_0", 8, 4, lambda o, j: r.g.at[:, o, beside_x[j], core, :, a_cols], r.g.at[:, pl.ds(0, 7), :, core, :, a_cols], r.sent.at[2], r.az_r, False, r.azp)
    bx = Ring("sp_1", 4, 8, lambda o, j: r.g.at[:, beside_z[j], o, core, :, b_cols], r.g.at[:, :, pl.ds(0, 3), core, :, b_cols], r.sent.at[3], r.bx_r, False, r.bxp)
    ny = Ring("tp", 4, 2, lambda o, j: r.normed.at[pl.ds(1 + o * 8 + j * 4, 4)], r.normed.at[pl.ds(0, 24)], r.sent.at[4], r.ny_r, True)

    def half_copies(c):
        return [
            pltpu.make_async_remote_copy(
                src_ref=ref, dst_ref=ref, send_sem=r.half_s.at[n], recv_sem=r.half_r.at[n], device_id={"sp_2": 1 - core}, device_id_type=MESH
            )
            for n, ref in enumerate((r.g.at[:, z, :, c, :, a_cols], r.g.at[:, :, x, c, :, b_cols]))
        ]

    def serve(*steps):
        for ring, step, i in steps:
            ring.service(step, i)

    def greeted():
        for c in weights:
            c.wait()
        wait_for_all()
        for i in (0, 1):
            ax.start(i)
            bz.start(i)
        az.start(0)

    def after_inside():
        serve((ax, 1, 0), (ax, 1, 1), (bz, 1, 0), (bz, 1, 1))

    def after_plane():
        for j in (1, 2):
            az.start(j)
            bx.start(j)

    def after_z():
        serve((ax, 2, 0))
        az.start(3)
        serve((az, 1, 0))

    mixer_phase(r, greeted, functools.partial(exchange, r, lambda: bx.start(0), after_inside, after_plane, after_z))

    for c in loads[len(EARLY) :]:
        c.wait()

    def project(b, n, slot):
        rows = pl.ds(pl.multiple_of(b * 128, 128), 128)
        return jnp.dot(r.act[rows, :], r.w_out[:, pl.ds(n * 512, 512)], preferred_element_type=F32)

    def while_projecting(slot):
        if slot == 0:
            serve((bz, 2, 0), (bz, 2, 1))
            bx.start(3)
            bx.start(4)
        elif slot == 1:
            serve((bx, 1, 0))

    first = RowSum(r.part1, r.far1, r.near1, r.own1, r.sent.at[5], r.sum1_r, functools.partial(finish_rows, r), project)
    first.others(while_projecting)
    first.mine()
    serve((az, 1, 1), (bx, 1, 1))
    first.pass_on()
    serve((az, 1, 2), (bx, 1, 2), (bz, 3, 0), (bz, 3, 1))
    bx.start(5)
    bx.start(6)
    serve((az, 1, 3), (bx, 2, 0), (az, 2, 0), (bx, 1, 3), (bx, 2, 1), (az, 2, 1), (bx, 1, 4), (bz, 4, 0))
    bx.start(7)
    for c in half_copies(core):
        c.start()
    first.arrived()

    def add_up(n, squares):
        cols = pl.ds(pl.multiple_of(n * 512, 512), 512)
        total = r.residual[:, cols].astype(F32) + first.total(n, ...)
        total = total.astype(BF16)
        r.stream[:, cols] = total
        total = total.astype(F32)
        return squares + total * total

    squares = lax.fori_loop(0, 4, add_up, jnp.zeros((128, 512), F32))
    scale = lax.rsqrt(jnp.sum(squares, axis=1, keepdims=True) / 2048 + 1e-06)

    def normalize(n, _):
        cols = pl.ds(pl.multiple_of(n * 256, 256), 256)
        v = (r.stream[:, cols].astype(F32) * scale * r.gain[:, cols]).astype(BF16)
        r.normed[pl.ds(1 + 8 * y, 8), :, cols] = v.reshape(8, 16, 256)
        return 0

    lax.fori_loop(0, 8, normalize, 0)
    ny.start(0)
    ny.start(1)
    halos = [
        pltpu.make_async_remote_copy(
            src_ref=r.normed.at[32], dst_ref=r.normed.at[0], send_sem=r.halo_s.at[q], recv_sem=r.halo_r.at[0],
            device_id=position(at + 1, q), device_id_type=MESH,
        )
        for q in range(4)
    ]
    ends = jnp.logical_and(y == 3, at < 63)

    @pl.when(ends)
    def _():
        for c in halos:
            c.start()

    serve((az, 2, 2), (bx, 2, 2), (az, 2, 3), (bx, 2, 3), (bx, 1, 5), (az, 3, 0), (bx, 2, 4), (bx, 1, 6), (az, 3, 1), (ny, 1, 0))
    serve((az, 3, 2), (bx, 1, 7), (bx, 2, 5), (az, 3, 3), (bx, 2, 6), (az, 4, 0), (az, 4, 1), (bx, 2, 7), (az, 4, 2), (az, 4, 3))
    for c in half_copies(1 - core):
        c.wait_recv()
    bx.shared_wait()
    az.shared_wait()
    pl.when(at > 0)(halos[0].wait_recv)
    serve((ny, 1, 1), (ny, 2, 0))

    def up(w):
        return jnp.dot(r.normed[...].reshape(528, 2048), w, preferred_element_type=F32).astype(BF16)

    def up_tile(n, _):
        m, cols = n % 2, pl.ds(pl.multiple_of((n // 2) * 256, 256), 256)
        r.pre[m, :, cols] = up(r.g[m, :, :, :, :, cols].reshape(2048, 256))
        return 0

    lax.fori_loop(0, 10, up_tile, 0, unroll=2)
    tail = pl.ds(1280, 128)
    last = up(jnp.concatenate([r.g[m, :, :, :, :, tail].reshape(2048, 128) for m in (0, 1)], axis=1))
    r.pre[0, :, tail], r.pre[1, :, tail] = last[:, :128], last[:, 128:]

    def convolved(b, m, cols):
        v = r.pre[m, pl.ds(pl.multiple_of(b * 128, 128), 144), cols].astype(F32)
        return sum(r.taps[k, pl.ds(m, 1), cols] * v[14 + k : 142 + k] for k in range(3))

    def hide(b, slot):
        def tile(n, _):
            cols = pl.ds(pl.multiple_of(n * 128, 128), 128)
            a, l = convolved(b, 0, cols), convolved(b, 1, cols)
            r.hidden[slot % 3, :, cols] = (a / (1.0 + jnp.exp(-a)) * l).astype(BF16)
            return 0

        lax.fori_loop(0, 11, tile, 0)

    def down(b, n, slot):
        w = r.g[2, pl.ds(2 * n, 2)].reshape(512, 1408)
        return lax.dot_general(w, r.hidden[slot % 3], NT, preferred_element_type=F32)

    second = RowSum(r.part2, r.far2, r.near2, r.own2, r.sent.at[6], r.sum2_r, hide, down)
    second.others(lambda slot: None)
    second.pass_on()
    second.mine()
    second.arrived()

    results = []
    for n in range(4):
        cols = pl.ds(n * 512, 512)
        total = jnp.transpose(second.total(n, ...))
        r.result[:, cols] = (r.stream[:, cols].astype(F32) + total).astype(BF16)
        results.append(pltpu.make_async_copy(r.result.at[:, cols], target.at[:, cols], r.load.at[3]))
        results[-1].start()
    for ring in (ax, bz, az, bx, ny):
        ring.drain()
    for c in half_copies(core):
        c.wait_send()
    first.drain()
    second.drain()

    @pl.when(ends)
    def _():
        for c in halos:
            c.wait_send()

    for c in results:
        c.wait()


def per_device(
    mixer_input, residual, log_step, rate_real, rate_imag, damping, in_map, out_map, skip, w_out, norm_gain, w_act, w_lin, conv_taps, w_down
):
    given = (
        mixer_input, damping.T, log_step[None], rate_real, rate_imag, in_map.transpose(0, 1, 3, 2), out_map, skip[None], residual,
        norm_gain[None], conv_taps.transpose(1, 0, 2), w_out, w_act, w_lin, w_down.T,
    )
    return pl.pallas_call(
        layer_kernel,
        out_shape=jax.ShapeDtypeStruct(residual.shape, BF16),
        in_specs=[pl.BlockSpec(memory_space=pl.ANY)] * len(given),
        out_specs=pl.BlockSpec(memory_space=pl.ANY),
        scratch_shapes=[pltpu.VMEM(*v) for v in IN_VMEM.values()] + list(SCRATCH.values()),
        compiler_params=pltpu.CompilerParams(collective_id=0, has_side_effects=True, vmem_limit_bytes=60 * 2**20),
        name="layer",
    )(*given)


def solution(mesh):
    split = Mesh(mesh.devices.reshape(8, 4, 2, mesh.shape["tp"]), ("sp_0", "sp_1", "sp_2", "tp"))
    in_specs = (
        P(SP, "tp"),
        P(SP_TP, None),
        P("tp"),
        P("tp", None),
        P("tp", None),
        P(SP, "tp"),
        P(None, "tp", None, None),
        P(None, "tp", None, None),
        P("tp"),
        P("tp", None),
        P(),
        P(SP, "tp"),
        P(SP, "tp"),
        P(None, None, "tp"),
        P("tp", SP),
    )
    out_specs = P(SP_TP, None)
    return jax.shard_map(
        per_device, mesh=split, in_specs=in_specs, out_specs=out_specs, check_vma=False
    )
```

time: 108 us -> 98.8 us (0.915); the launches traced: 106 us -> 98.7 us
  Pallas kernels: 102 us -> 96.8 us
  local copies, waits for them, and re-layouts: 3.21 us -> 1.88 us
    pallas_call x1, Pallas kernels: 102 us -> 96.8 us  [per_device(): pl.pallas_call(layer_kernel, out_shape=jax.ShapeDtypeStruct(residual.shap...]
    broadcast_in_dim x1 -> x0, local copies, waits for them, and re-layouts: 1.33 us -> none  [per_device(): jnp.broadcast_to(log_step[:, None], rate_real.shape)]
where the time goes in v3:
time: 98.8 us; the launch traced here: 98.7 us
  Pallas kernels  96.8 us (98%)
  local copies, waits for them, and re-layouts  1.88 us (2%)
    pallas_call x1, Pallas kernels, per_device(): pl.pallas_call(layer_kernel, out_shape=jax.ShapeDtypeStruct(residual.shap...  96.8 us

profile of v3, /device:TPU:1, one launch (start us, length us, event | category | flops | bytes accessed | tf_op | source)
XLA Modules:
  0.0 98.7 jit_solution(4600036484247736545)
XLA Ops:
  0.0 96.8 %layer.1 = bf16[128,2048]{1,0:T(8,128)(2,1)} custom-call(bf16[512,512]{1,0:T(8,128)(2,1)} %refs_0_.1, f32[32,512]{1,0:T(8,128)} %bitcast.9, f32[1,32]{1,0:T(1,128)} %bitcast.13, f32[32,64]{1,0:T(8,128)} %refs_3_.1, f32[32,64]{1,0:T(8,128)} %refs_4_.1, f32[2,32,16,64]{3,2,1,0:T(8,128)} %bitcast.7, f32[2,32,16,64]{3,2,1,0:T(8,128)} %refs_6_.1, ...), custom_call_target="tpu_custom_call" | custom-call | tf_op jit(solution)/shard_map/layer/pallas_call | solution.py:648
  96.8 1.9 %copy.17 = bf16[128,2048]{1,0:T(8,128)(2,1)} copy(bf16[128,2048]{1,0:T(8,128)(2,1)} %layer.1) | data formatting | bytes 1048576

commit v4 on v3

--- a/solution.py
+++ b/solution.py
@@ -450,10 +450,7 @@
     for c in loads[: len(EARLY)] + weights + loads[len(EARLY) :]:
         c.start()
     r.got_z[...] = jnp.zeros_like(r.got_z)
-    @pl.when(at == 0)
-    def _():
-        r.normed[0] = jnp.zeros((16, 2048), BF16)
-
+    r.normed[0] = jnp.zeros((16, 2048), BF16)
     peers = [in_plane(x * 2 + core + d) for d in range(1, 8)]
     peers += [{axis: lax.rem(lax.axis_index(axis) + d, count)} for axis, count in (("sp_0", 8), ("tp", 4)) for d in range(1, count)]
     peers += [position(at + n, q) for n in (1, 63) for q in range(4)]
@@ -554,11 +551,9 @@
         return 0
 
     lax.fori_loop(0, 8, normalize, 0)
-    ny.start(0)
-    ny.start(1)
     halos = [
         pltpu.make_async_remote_copy(
-            src_ref=r.normed.at[32], dst_ref=r.normed.at[0], send_sem=r.halo_s.at[q], recv_sem=r.halo_r.at[0],
+            src_ref=r.normed.at[32, pl.ds(8, 8)], dst_ref=r.normed.at[0, pl.ds(8, 8)], send_sem=r.halo_s.at[q], recv_sem=r.halo_r.at[0],
             device_id=position(at + 1, q), device_id_type=MESH,
         )
         for q in range(4)
@@ -570,40 +565,51 @@
         for c in halos:
             c.start()
 
-    serve((az, 2, 2), (bx, 2, 2), (az, 2, 3), (bx, 2, 3), (bx, 1, 5), (az, 3, 0), (bx, 2, 4), (bx, 1, 6), (az, 3, 1), (ny, 1, 0))
-    serve((az, 3, 2), (bx, 1, 7), (bx, 2, 5), (az, 3, 3), (bx, 2, 6), (az, 4, 0), (az, 4, 1), (bx, 2, 7), (az, 4, 2), (az, 4, 3))
+    ny.start(0)
+    ny.start(1)
+    serve((az, 2, 2), (bx, 2, 2), (az, 2, 3), (bx, 2, 3), (bx, 1, 5), (bx, 1, 6), (az, 3, 0), (bx, 2, 4), (bx, 1, 7), (az, 3, 1), (ny, 1, 0))
+    serve((bx, 2, 5), (az, 3, 2), (bx, 2, 6), (az, 3, 3), (bx, 2, 7), (az, 4, 0), (az, 4, 1), (az, 4, 2), (az, 4, 3))
     for c in half_copies(1 - core):
         c.wait_recv()
+    pl.when(at > 0)(halos[0].wait_recv)
     bx.shared_wait()
-    az.shared_wait()
-    pl.when(at > 0)(halos[0].wait_recv)
     serve((ny, 1, 1), (ny, 2, 0))
 
     def up(w):
         return jnp.dot(r.normed[...].reshape(528, 2048), w, preferred_element_type=F32).astype(BF16)
 
-    def up_tile(n, _):
-        m, cols = n % 2, pl.ds(pl.multiple_of((n // 2) * 256, 256), 256)
+    def up_tile(first, n, _):
+        m, cols = n % 2, pl.ds(pl.multiple_of(first + (n // 2) * 256, 128), 256)
         r.pre[m, :, cols] = up(r.g[m, :, :, :, :, cols].reshape(2048, 256))
         return 0
 
-    lax.fori_loop(0, 10, up_tile, 0, unroll=2)
-    tail = pl.ds(1280, 128)
-    last = up(jnp.concatenate([r.g[m, :, :, :, :, tail].reshape(2048, 128) for m in (0, 1)], axis=1))
-    r.pre[0, :, tail], r.pre[1, :, tail] = last[:, :128], last[:, 128:]
+    lax.fori_loop(0, 6, functools.partial(up_tile, 640), 0, unroll=2)
+    az.shared_wait()
+    lax.fori_loop(0, 4, functools.partial(up_tile, 0), 0, unroll=2)
+    tail = pl.ds(512, 128)
+
+    def up_tail(m, _):
+        r.pre[m, :, tail] = up(r.g[m, :, :, :, :, tail].reshape(2048, 128))
+        return 0
+
+    lax.fori_loop(0, 2, up_tail, 0, unroll=2)
 
     def convolved(b, m, cols):
         v = r.pre[m, pl.ds(pl.multiple_of(b * 128, 128), 144), cols].astype(F32)
         return sum(r.taps[k, pl.ds(m, 1), cols] * v[14 + k : 142 + k] for k in range(3))
 
     def hide(b, slot):
-        def tile(n, _):
-            cols = pl.ds(pl.multiple_of(n * 128, 128), 128)
+        def tile(cols):
             a, l = convolved(b, 0, cols), convolved(b, 1, cols)
             r.hidden[slot % 3, :, cols] = (a / (1.0 + jnp.exp(-a)) * l).astype(BF16)
+
+        def pair(n, _):
+            for half in (0, 1):
+                tile(pl.ds(pl.multiple_of(n * 256 + half * 128, 128), 128))
             return 0
 
-        lax.fori_loop(0, 11, tile, 0)
+        lax.fori_loop(0, 5, pair, 0)
+        tile(pl.ds(1280, 128))
 
     def down(b, n, slot):
         w = r.g[2, pl.ds(2 * n, 2)].reshape(512, 1408)
@@ -613,10 +619,11 @@
     second.others(lambda slot: None)
     second.pass_on()
     second.mine()
-    second.arrived()
-
+    for c in second.nears:
+        c.wait_recv()
     results = []
-    for n in range(4):
+    for n in (0, 2, 1, 3):
+        second.sums[n].wait_recv()
         cols = pl.ds(n * 512, 512)
         total = jnp.transpose(second.total(n, ...))
         r.result[:, cols] = (r.stream[:, cols].astype(F32) + total).astype(BF16)

time: 98.8 us -> 95.9 us (0.971)
  the two profiles are of different devices: /device:TPU:1 before, /device:TPU:102 now
where the time goes in v4:
time: 95.9 us; the launch traced here: 95.8 us
  Pallas kernels  93.9 us (98%)
  local copies, waits for them, and re-layouts  1.88 us (2%)
    pallas_call x1, Pallas kernels, per_device(): pl.pallas_call(layer_kernel, out_shape=jax.ShapeDtypeStruct(residual.shap...  93.9 us

profile of v4, /device:TPU:102, one launch (start us, length us, event | category | flops | bytes accessed | tf_op | source)
XLA Modules:
  0.0 95.8 jit_solution(16119691495982980461)
XLA Ops:
  0.0 93.9 %layer.1 = bf16[128,2048]{1,0:T(8,128)(2,1)} custom-call(bf16[512,512]{1,0:T(8,128)(2,1)} %refs_0_.1, f32[32,512]{1,0:T(8,128)} %bitcast.9, f32[1,32]{1,0:T(1,128)} %bitcast.13, f32[32,64]{1,0:T(8,128)} %refs_3_.1, f32[32,64]{1,0:T(8,128)} %refs_4_.1, f32[2,32,16,64]{3,2,1,0:T(8,128)} %bitcast.7, f32[2,32,16,64]{3,2,1,0:T(8,128)} %refs_6_.1, ...), custom_call_target="tpu_custom_call" | custom-call | tf_op jit(solution)/shard_map/layer/pallas_call | solution.py:655
  93.9 1.9 %copy.17 = bf16[128,2048]{1,0:T(8,128)(2,1)} copy(bf16[128,2048]{1,0:T(8,128)(2,1)} %layer.1) | data formatting | bytes 1048576

commit v5 on v4

--- a/solution.py
+++ b/solution.py
@@ -85,7 +85,6 @@
     for k in range(PAIRS):
         r.e7[pl.ds(k, CH, stride=PAIRS), :] = jnp.where(low, ends[:, 2 * k : 2 * k + 1], ends[:, 2 * k + 1 : 2 * k + 2])
 
-    r.ex[...] = spread_out(jnp.exp(d))
     shrink = spread_out(jnp.exp(-d)) * r.u[...].astype(F32)
     for j in range(4):
         r.v[j] = shrink[:, j * 128 : j * 128 + 128]
@@ -161,8 +160,10 @@
         return 0
 
     def inside_part(n):
-        cuts = (0, 10, 16)
+        cuts = (0, 12, 16)
         lax.fori_loop(cuts[n], cuts[n + 1], inside, 0, unroll=2)
+        if n == 0:
+            r.ex[...] = spread_out(jnp.exp(d))
 
     vr, vi = comm(ar, ai, vr, vi, e_all, inside_part)
     lax.fori_loop(0, CH, functools.partial(advance, keep=True), (vr, vi, one), unroll=8)
@@ -239,7 +240,7 @@
     return lambda: pl.semaphore_wait(barrier, len(peers))
 
 
-def exchange(r, after_own, after_inside, after_plane, after_z, ar, ai, vr, vi, e, part):
+def exchange(r, after_own, after_inside, after_plane, ar, ai, vr, vi, e, part):
     at, z = lax.axis_index("sp_1") * 2 + lax.axis_index("sp_2"), lax.axis_index("sp_0")
 
     def copy(level, d, got, peer):
@@ -281,7 +282,6 @@
         pl.when(z + d < 8)(sends[d - 1].start)
     after_plane()
     part(1)
-    after_z()
     for d in range(1, 8):
         pl.when(z + d < 8)(sends[d - 1].wait_send)
         pl.when(z >= d)(sends[d - 1].wait_recv)
@@ -497,12 +497,7 @@
             az.start(j)
             bx.start(j)
 
-    def after_z():
-        serve((ax, 2, 0))
-        az.start(3)
-        serve((az, 1, 0))
-
-    mixer_phase(r, greeted, functools.partial(exchange, r, lambda: bx.start(0), after_inside, after_plane, after_z))
+    mixer_phase(r, greeted, functools.partial(exchange, r, lambda: bx.start(0), after_inside, after_plane))
 
     for c in loads[len(EARLY) :]:
         c.wait()
@@ -516,6 +511,9 @@
             serve((bz, 2, 0), (bz, 2, 1))
             bx.start(3)
             bx.start(4)
+            serve((ax, 2, 0))
+            az.start(3)
+            serve((az, 1, 0))
         elif slot == 1:
             serve((bx, 1, 0))
 
@@ -527,10 +525,7 @@
     serve((az, 1, 2), (bx, 1, 2), (bz, 3, 0), (bz, 3, 1))
     bx.start(5)
     bx.start(6)
-    serve((az, 1, 3), (bx, 2, 0), (az, 2, 0), (bx, 1, 3), (bx, 2, 1), (az, 2, 1), (bx, 1, 4), (bz, 4, 0))
-    bx.start(7)
-    for c in half_copies(core):
-        c.start()
+    serve((az, 1, 3), (bx, 2, 0), (az, 2, 0), (bx, 1, 3), (bx, 2, 1), (az, 2, 1), (bx, 1, 4))
     first.arrived()
 
     def add_up(n, squares):
@@ -567,8 +562,12 @@
 
     ny.start(0)
     ny.start(1)
+    serve((bz, 4, 0))
+    bx.start(7)
+    for c in half_copies(core):
+        c.start()
     serve((az, 2, 2), (bx, 2, 2), (az, 2, 3), (bx, 2, 3), (bx, 1, 5), (bx, 1, 6), (az, 3, 0), (bx, 2, 4), (bx, 1, 7), (az, 3, 1), (ny, 1, 0))
-    serve((bx, 2, 5), (az, 3, 2), (bx, 2, 6), (az, 3, 3), (bx, 2, 7), (az, 4, 0), (az, 4, 1), (az, 4, 2), (az, 4, 3))
+    serve((bx, 2, 5), (az, 3, 2), (bx, 2, 6), (bx, 2, 7), (az, 3, 3), (az, 4, 0), (az, 4, 1), (az, 4, 2), (az, 4, 3))
     for c in half_copies(1 - core):
         c.wait_recv()
     pl.when(at > 0)(halos[0].wait_recv)

time: 95.9 us -> 96.2 us (level)
  the two profiles are of different devices: /device:TPU:102 before, /device:TPU:70 now
where the time goes in v5:
time: 96.2 us; the launch traced here: 96.1 us
  Pallas kernels  94.2 us (98%)
  local copies, waits for them, and re-layouts  1.88 us (2%)
    pallas_call x1, Pallas kernels, per_device(): pl.pallas_call(layer_kernel, out_shape=jax.ShapeDtypeStruct(residual.shap...  94.2 us

profile of v5, /device:TPU:70, one launch (start us, length us, event | category | flops | bytes accessed | tf_op | source)
XLA Modules:
  0.0 96.1 jit_solution(1965375714434644726)
XLA Ops:
  0.0 94.2 %layer.1 = bf16[128,2048]{1,0:T(8,128)(2,1)} custom-call(bf16[512,512]{1,0:T(8,128)(2,1)} %refs_0_.1, f32[32,512]{1,0:T(8,128)} %bitcast.9, f32[1,32]{1,0:T(1,128)} %bitcast.13, f32[32,64]{1,0:T(8,128)} %refs_3_.1, f32[32,64]{1,0:T(8,128)} %refs_4_.1, f32[2,32,16,64]{3,2,1,0:T(8,128)} %bitcast.7, f32[2,32,16,64]{3,2,1,0:T(8,128)} %refs_6_.1, ...), custom_call_target="tpu_custom_call" | custom-call | tf_op jit(solution)/shard_map/layer/pallas_call | solution.py:654
  94.2 1.9 %copy.17 = bf16[128,2048]{1,0:T(8,128)(2,1)} copy(bf16[128,2048]{1,0:T(8,128)(2,1)} %layer.1) | data formatting | bytes 1048576
